TPU v7x, 1024 devices: a whole 4x4x32 slice. The times are simulated.
1024 devices in a mesh: tp: 128 (over z, y), dp: 8 (over x, core).
Axes of the slice: x: 4, y: 4, z: 32, core: 2. Of those that a mesh axis runs over, the one named last changes fastest.
Arguments:
- incoming_token: bfloat16 [256, 4096], P(None, 'dp'), may hold values from -60 to 60
- input_norm_gain: float32 [2, 4096], P(None, 'dp'), may hold values from 0.1 to 1.9
- receptance_weight: bfloat16 [2, 4096, 8192], P(None, 'dp', 'tp'), may hold values from -0.09375 to 0.09375
- key_weight: bfloat16 [2, 4096, 8192], P(None, 'dp', 'tp'), may hold values from -0.09375 to 0.09375
- value_weight: bfloat16 [2, 4096, 8192], P(None, 'dp', 'tp'), may hold values from -0.09375 to 0.09375
- decay_weight: bfloat16 [2, 4096, 8192], P(None, 'dp', 'tp'), may hold values from -0.09375 to 0.09375
- learning_rate_weight: bfloat16 [2, 4096, 8192], P(None, 'dp', 'tp'), may hold values from -0.09375 to 0.09375
- gate_weight: bfloat16 [2, 4096, 8192], P(None, 'dp', 'tp'), may hold values from -0.09375 to 0.09375
- channel_decay_floor: float32 [2, 8192], P(None, 'tp'), may hold values from -5 to 2
- direct_token_weight: float32 [2, 8192], P(None, 'tp'), may hold values from -0.6 to 0.6
- head_norm_gain: float32 [2, 8192], P(None, 'tp'), may hold values from 0.1 to 1.9
- output_weight: bfloat16 [2, 8192, 4096], P(None, 'tp', 'dp'), may hold values from -0.0625 to 0.0625
- incoming_state: float32 [2, 256, 128, 64, 64], P(None, 'dp', 'tp'), may hold values from -6 to 6
Outputs:
- hidden_out: bfloat16 [256, 4096], P(None, 'dp')
- state_out: float32 [2, 256, 128, 64, 64], P(None, 'dp', 'tp')
All inputs are finite; a program needn't handle non-finite values.
Results may differ from a plain program's by a relative error of at most 0.0053.
Values may be sent and summed in bfloat16 or wider, within the bound.
A program may use at most 32 MiB of HBM per device.

v0:
```python
import jax
import jax.numpy as jnp
from jax import lax
from jax.sharding import Mesh
from jax.sharding import PartitionSpec as P

D = 4096
HEAD_CHANNELS = 64
TP = ("tp_0", "tp_1")


def sent_to_all(array, axis):
    copies = jnp.broadcast_to(array, (lax.axis_size(axis), *array.shape))
    return lax.all_to_all(copies, axis, split_axis=0, concat_axis=0, tiled=True)


def of_everyone(array, axis):
    everything = sent_to_all(array, axis)
    return jnp.sum(everything, axis=0)


def cut_along(array, dim, size):
    dims = array.shape
    parts = array.reshape(*dims[:dim], size, dims[dim] // size, *dims[dim + 1 :])
    return jnp.moveaxis(parts, dim, 0)


def sent_and_summed(array, axis, dim):
    parts = cut_along(array, dim, lax.axis_size(axis))
    arrived = lax.all_to_all(parts, axis, split_axis=0, concat_axis=0, tiled=True)
    return arrived.sum(axis=0)


def joined_along(parts, dim):
    parts = jnp.moveaxis(parts, 0, dim)
    dims = parts.shape
    return parts.reshape(*dims[:dim], dims[dim] * dims[dim + 1], *dims[dim + 2 :])


def gather_directly(array, axis, dim):
    return joined_along(sent_to_all(array, axis), dim)


def scatter_axes(array, axes, dim):
    if not axes:
        return array
    nearer = lax.psum_scatter(array, axes[0], scatter_dimension=dim, tiled=True)
    return scatter_axes(nearer, axes[1:], dim)


def all_blocks(array, axes, sequence):
    parts = array
    for k in sequence:
        parts = lax.all_gather(parts, axes[k])
    done = sequence[::-1]
    back = [done.index(k) for k in range(len(axes))]
    parts = parts.transpose(*back, *range(len(axes), parts.ndim))
    return parts.reshape(-1, *array.shape)


def whole_of(array, axes, sequence, dim):
    return joined_along(all_blocks(array, axes, sequence), dim)


def recurrent_mix_heads(
    projected_output, earlier_state, channel_decay_floor, direct_token_weight, head_norm_gain
):
    step_count = projected_output.shape[0]
    local_heads = channel_decay_floor.shape[0] // HEAD_CHANNELS
    sections = projected_output.reshape(step_count, 6, local_heads, HEAD_CHANNELS)
    receptance_rows, keyvec, value_vector, pre_decay, pre_rate, pre_gate = [
        sections[:, part_index] for part_index in range(6)
    ]
    decay_pre = channel_decay_floor.reshape(local_heads, HEAD_CHANNELS) + pre_decay
    decay_factor = jnp.exp(-jnp.exp(-jax.nn.softplus(-decay_pre) - 0.5))
    learn_rate = jax.nn.sigmoid(pre_rate)
    output_gate_value = jax.nn.sigmoid(pre_gate)
    unit_key = keyvec * lax.rsqrt(jnp.sum(keyvec * keyvec, axis=-1, keepdims=True) + 1e-06)
    rescaled_key = keyvec * learn_rate
    removed = -jnp.einsum("shvk,shk->shv", earlier_state, unit_key, precision=lax.Precision.HIGHEST)
    refreshed_state = (
        earlier_state * decay_factor[:, :, None, :]
        + removed[..., None] * (unit_key * learn_rate)[:, :, None, :]
        + value_vector[..., None] * rescaled_key[:, :, None, :]
    )
    readout = jnp.einsum(
        "shvk,shk->shv", refreshed_state, receptance_rows, precision=lax.Precision.HIGHEST
    )
    group_mean = jnp.mean(readout, axis=-1, keepdims=True)
    group_var = jnp.mean(jnp.square(readout - group_mean), axis=-1, keepdims=True)
    normalized_input = (
        (readout - group_mean)
        * lax.rsqrt(group_var + 0.00064)
        * head_norm_gain.reshape(local_heads, HEAD_CHANNELS)
    )
    direct_token_term = (
        jnp.sum(
            receptance_rows
            * rescaled_key
            * direct_token_weight.reshape(local_heads, HEAD_CHANNELS),
            axis=-1,
            keepdims=True,
        )
        * value_vector
    )
    mixer_output = (
        ((normalized_input + direct_token_term) * output_gate_value)
        .reshape(step_count, local_heads * HEAD_CHANNELS)
        .astype(jnp.bfloat16)
    )
    return (mixer_output, refreshed_state)


def per_device(
    incoming_token,
    input_norm_gain,
    receptance_weight,
    key_weight,
    value_weight,
    decay_weight,
    learning_rate_weight,
    gate_weight,
    channel_decay_floor,
    direct_token_weight,
    head_norm_gain,
    output_weight,
    incoming_state,
):
    hidden = incoming_token
    seq_dev = incoming_state.shape[1]
    dp_start = lax.axis_index("dp") * seq_dev
    new_states = []
    for block_index in range(2):
        hidden_wide = hidden.astype(jnp.float32)
        partial_squares = jnp.sum(hidden_wide * hidden_wide, axis=1)
        scaled_in = (hidden_wide * input_norm_gain[block_index]).astype(jnp.bfloat16)
        matrices = (
            receptance_weight[block_index],
            key_weight[block_index],
            value_weight[block_index],
            decay_weight[block_index],
            learning_rate_weight[block_index],
            gate_weight[block_index],
        )
        square_total = of_everyone(partial_squares, "dp")
        own_squares = lax.dynamic_slice_in_dim(square_total, dp_start, seq_dev, 0)
        summed = sent_and_summed(
            jnp.concatenate(
                [
                    jnp.dot(scaled_in, matrix, preferred_element_type=jnp.float32)
                    for matrix in matrices
                ],
                axis=1,
            ),
            "dp",
            0,
        )
        projected_output = summed * lax.rsqrt(own_squares[:, None] / D + 1e-06)
        mixer_output, refreshed_state = recurrent_mix_heads(
            projected_output,
            incoming_state[block_index],
            channel_decay_floor[block_index],
            direct_token_weight[block_index],
            head_norm_gain[block_index],
        )
        new_states.append(refreshed_state)
        out_matrix = output_weight[block_index]
        branch = jnp.dot(
            gather_directly(mixer_output, "dp", 0), out_matrix, preferred_element_type=jnp.float32
        )
        share_rows = branch.shape[0] // lax.axis_size(TP)
        branch_share = scatter_axes(branch, TP, 0)
        residual_part = lax.dynamic_slice_in_dim(
            hidden_wide, lax.axis_index(TP) * share_rows, share_rows, 0
        )
        hidden = whole_of((residual_part + branch_share).astype(jnp.bfloat16), TP, (0, 1), 0)
    return (hidden, jnp.stack(new_states))


def solution(mesh):
    finer = Mesh(mesh.devices.reshape(32, 4, mesh.shape["dp"]), ("tp_0", "tp_1", "dp"))
    return jax.shard_map(
        per_device,
        mesh=finer,
        in_specs=(
            P(None, "dp"),
            P(None, "dp"),
            P(None, "dp", TP),
            P(None, "dp", TP),
            P(None, "dp", TP),
            P(None, "dp", TP),
            P(None, "dp", TP),
            P(None, "dp", TP),
            P(None, TP),
            P(None, TP),
            P(None, TP),
            P(None, TP, "dp"),
            P(None, "dp", TP, None, None),
        ),
        out_specs=(P(None, "dp"), P(None, "dp", TP, None, None)),
        check_vma=False,
    )
```

profile of v0, /device:TPU:2, one launch (start us, length us, event | category | flops | bytes accessed | tf_op | source)
XLA Modules:
  0.0 535.6 jit_solution(4195271199215618587)
XLA Ops:
  7.2 1.1 multiply_reduce_fusion.1
  8.9 16.4 %all-to-all-start.1 = ((f32[8,1,256]{2,1,0:T(1,128)}), f32[8,1,256]{2,1,0:T(1,128)S(1)}, u32[]{:S(2)}, u32[]{:S(2)}) async-start(f32[8,1,256]{2,1,0:T(1,128)} %broadcast_in_dim.10), calls=%async_computation.1 | async-start | bytes 16384 | tf_op jit(solution)/shard_map/all_to_all | solution.py:14
  25.3 1.3 fusion.102
  26.7 1.2 convolution_dynamic-update-slice_fusion.11
  27.8 1.2 convolution_dynamic-update-slice_fusion.10
  29.0 1.2 convolution_dynamic-update-slice_fusion.9
  30.2 1.3 convolution_dynamic-update-slice_fusion.8
  31.5 1.2 convolution_dynamic-update-slice_fusion.7
  34.4 4.8 all-to-all-start
  40.4 6.3 %all-to-all-done = f32[8,32,384]{2,1,0:T(8,128)S(1)} async-done(((f32[8,32,384]{2,1,0:T(8,128)}), f32[8,32,384]{2,1,0:T(8,128)S(1)}, u32[]{:S(2)}, u32[]{:S(2)}) %all-to-all-start) | async-done | bytes 393248 | tf_op jit(solution)/shard_map/all_to_all | solution.py:30
  47.3 1.7 fusion.6
  49.0 2.1 fusion.10
  51.7 7.8 %all_to_all.32 = bf16[8,2,1024]{2,1,0:T(2,128)(2,1)S(1)} all-to-all(bf16[8,2,1024]{2,1,0:T(2,128)(2,1)S(1)} %reshape.621), channel_id=1, replica_groups=mesh['tp_0'=32,'tp_1'=4,'dp'=8] {'dp'}, dimensions={0} | all-to-all | bytes 65536 | tf_op jit(solution)/shard_map/all_to_all | solution.py:14
  60.8 1.3 dynamic-slice
  62.6 128.2 %reduce-scatter.3.cloned.1.call-done = f32[8,512]{1,0:T(8,128)} async-done(((f32[256,512]{1,0:T(8,128)}), f32[8,512]{1,0:T(8,128)}) %reduce-scatter.3.cloned.1.call-update) | async-done | bytes 16400 | tf_op jit(solution)/shard_map/reduce_scatter | solution.py:47
  190.8 17.5 %all-reduce = f32[8,512]{1,0:T(8,128)S(1)} all-reduce(f32[8,512]{1,0:T(8,128)} %reduce-scatter.3.cloned.1.call-done), channel_id=7, replica_groups=mesh['tp_0'=32,'tp_1'=4,'dp'=8] {'tp_1'}, use_global_device_ids=true, to_apply=%region_8.9.clone | all-reduce | flops 4096 | bytes 32768
  208.3 52.9 %all-gather.4 = bf16[32,2,512]{2,1,0:T(2,128)(2,1)S(1)} all-gather(bf16[1,2,512]{2,1,0:T(2,128)(2,1)S(1)} %fusion.100), channel_id=2, replica_groups=mesh['tp_0'=32,'tp_1'=4,'dp'=8] {'tp_0'}, dimensions={0}, use_global_device_ids=true | all-gather | bytes 67584 | tf_op jit(solution)/shard_map/all_gather | solution.py:54
  261.2 12.4 %all-gather.1 = bf16[128,2,512]{2,1,0:T(2,128)(2,1)S(1)} all-gather(bf16[32,2,512]{2,1,0:T(2,128)(2,1)S(1)} %all-gather.4), channel_id=3, replica_groups=mesh['tp_0'=32,'tp_1'=4,'dp'=8] {'tp_1'}, dimensions={0}, use_global_device_ids=true | all-gather | bytes 327680 | tf_op jit(solution)/shard_map/all_gather | solution.py:54
  274.8 4.8 all-to-all-start.4
  284.0 1.0 convolution_dynamic-update-slice_fusion.1
  285.1 1.0 convolution_dynamic-update-slice_fusion
  287.0 4.8 all-to-all-start.3
  292.6 6.6 %all-to-all-done.3 = f32[8,32,384]{2,1,0:T(8,128)S(1)} async-done(((f32[8,32,384]{2,1,0:T(8,128)}), f32[8,32,384]{2,1,0:T(8,128)S(1)}, u32[]{:S(2)}, u32[]{:S(2)}) %all-to-all-start.3) | async-done | bytes 393248 | tf_op jit(solution)/shard_map/all_to_all | solution.py:30
  301.2 1.7 fusion
  303.6 2.1 fusion.4
  306.2 7.8 %all_to_all.33 = bf16[8,2,1024]{2,1,0:T(2,128)(2,1)S(1)} all-to-all(bf16[8,2,1024]{2,1,0:T(2,128)(2,1)S(1)} %reshape.623), channel_id=1, replica_groups=mesh['tp_0'=32,'tp_1'=4,'dp'=8] {'dp'}, dimensions={0} | all-to-all | bytes 65536 | tf_op jit(solution)/shard_map/all_to_all | solution.py:14
  316.0 1.4 multiply_add_fusion.1
  317.5 1.5 pad_maximum_fusion
  319.0 126.2 %reduce-scatter.5.cloned.1.call-done = f32[8,512]{1,0:T(8,128)} async-done(((f32[256,512]{1,0:T(8,128)}), f32[8,512]{1,0:T(8,128)}) %reduce-scatter.5.cloned.1.call-update) | async-done | bytes 16400 | tf_op jit(solution)/shard_map/reduce_scatter | solution.py:47
  445.2 17.5 %all-reduce.1 = f32[8,512]{1,0:T(8,128)S(1)} all-reduce(f32[8,512]{1,0:T(8,128)} %reduce-scatter.5.cloned.1.call-done), channel_id=9, replica_groups=mesh['tp_0'=32,'tp_1'=4,'dp'=8] {'tp_1'}, use_global_device_ids=true, to_apply=%region_17.18.clone | all-reduce | flops 4096 | bytes 32768
  462.6 52.9 %all-gather.5 = bf16[32,2,512]{2,1,0:T(2,128)(2,1)S(1)} all-gather(bf16[1,2,512]{2,1,0:T(2,128)(2,1)S(1)} %fusion.101), channel_id=4, replica_groups=mesh['tp_0'=32,'tp_1'=4,'dp'=8] {'tp_0'}, dimensions={0}, use_global_device_ids=true | all-gather | bytes 67584 | tf_op jit(solution)/shard_map/all_gather | solution.py:54
  515.5 12.2 %all-gather.3 = bf16[128,2,512]{2,1,0:T(2,128)(2,1)S(1)} all-gather(bf16[32,2,512]{2,1,0:T(2,128)(2,1)S(1)} %all-gather.5), channel_id=5, replica_groups=mesh['tp_0'=32,'tp_1'=4,'dp'=8] {'tp_1'}, dimensions={0}, use_global_device_ids=true | all-gather | bytes 327680 | tf_op jit(solution)/shard_map/all_gather | solution.py:54
  (111 shorter events, 19.1 us)
Async XLA Ops:
  7.2 25.5 %copy-start.1 = (bf16[256,512]{1,0:T(8,128)(2,1)S(1)}, bf16[256,512]{1,0:T(8,128)(2,1)}, u32[]{:S(2)}) copy-start(bf16[256,512]{1,0:T(8,128)(2,1)} %param.13) | copy-start | bytes 786436
  7.2 25.5 %copy-start.14 = (bf16[2,512,64]{1,2,0:T(8,128)(2,1)S(1)}, bf16[2,512,64]{1,2,0:T(8,128)(2,1)}, u32[]{:S(2)}) copy-start(bf16[2,512,64]{1,2,0:T(8,128)(2,1)} %param.20) | copy-start | bytes 393220
  7.2 25.7 %copy-start.16 = (f32[2,64]{1,0:T(2,128)S(1)}, f32[2,64]{1,0:T(2,128)}, u32[]{:S(2)}) copy-start(f32[2,64]{1,0:T(2,128)} %param.21) | copy-start | bytes 1540
  8.9 25.5 %all-to-all-start.1 = ((f32[8,1,256]{2,1,0:T(1,128)}), f32[8,1,256]{2,1,0:T(1,128)S(1)}, u32[]{:S(2)}, u32[]{:S(2)}) async-start(f32[8,1,256]{2,1,0:T(1,128)} %broadcast_in_dim.10), calls=%async_computation.1 | async-start | bytes 16384 | tf_op jit(solution)/shard_map/all_to_all | solution.py:14
  26.7 12.6 %copy-start.17 = (f32[2,64]{1,0:T(2,128)S(1)}, f32[2,64]{1,0:T(2,128)}, u32[]{:S(2)}) copy-start(f32[2,64]{1,0:T(2,128)} %param.22) | copy-start | bytes 1540
  26.7 13.1 %copy-start.18 = (f32[2,64]{1,0:T(2,128)S(1)}, f32[2,64]{1,0:T(2,128)}, u32[]{:S(2)}) copy-start(f32[2,64]{1,0:T(2,128)} %param.23) | copy-start | bytes 1540
  30.2 17.1 %copy-start = (f32[2,32,1,64,64]{4,3,2,1,0:T(8,128)S(1)}, f32[2,32,1,64,64]{4,3,2,1,0:T(8,128)}, u32[]{:S(2)}) copy-start(f32[2,32,1,64,64]{4,3,2,1,0:T(8,128)} %param.25) | copy-start | bytes 3145732
  34.4 12.3 %all-to-all-start = ((f32[8,32,384]{2,1,0:T(8,128)}), f32[8,32,384]{2,1,0:T(8,128)S(1)}, u32[]{:S(2)}, u32[]{:S(2)}) async-start(f32[8,32,384]{2,1,0:T(8,128)} %bitcast.9), calls=%async_computation | async-start | bytes 786432 | tf_op jit(solution)/shard_map/all_to_all | solution.py:30
  39.2 151.6 %reduce-scatter.3.cloned.1.call-start = ((), (), s32[]{:S(2)}) async-start(), calls=%async_computation.8 | async-start | bytes 540672 | tf_op jit(solution)/shard_map/reduce_scatter | solution.py:47
  46.7 12.9 %copy-start.2 = (bf16[2,64,512]{2,1,0:T(8,128)(2,1)S(1)}, bf16[2,64,512]{2,1,0:T(8,128)(2,1)}, u32[]{:S(2)}) copy-start(bf16[2,64,512]{2,1,0:T(8,128)(2,1)} %param.24) | copy-start | bytes 393220
  47.0 4.6 copy-start.3
  47.0 13.6 %copy-start.5 = (f32[32,64]{1,0:T(8,128)}, f32[32,64]{1,0:T(8,128)S(1)}, u32[]{:S(2)}) copy-start(f32[32,64]{1,0:T(8,128)S(1)} %get-tuple-element.16) | copy-start | bytes 24580
  47.1 13.6 %copy-start.7 = (f32[32,64]{1,0:T(8,128)}, f32[32,64]{1,0:T(8,128)S(1)}, u32[]{:S(2)}) copy-start(f32[32,64]{1,0:T(8,128)S(1)} %multiply_bitcast_fusion.1) | copy-start | bytes 24580
  49.0 11.6 %copy-start.9 = (f32[32,64]{1,0:T(8,128)}, f32[32,64]{1,0:T(8,128)S(1)}, u32[]{:S(2)}) copy-start(f32[32,64]{1,0:T(8,128)S(1)} %neg.103) | copy-start | bytes 24580
  261.2 19.5 %copy-start.13 = (bf16[2,512,64]{1,2,0:T(8,128)(2,1)S(1)}, bf16[2,512,64]{1,2,0:T(8,128)(2,1)}, u32[]{:S(2)}) copy-start(bf16[2,512,64]{1,2,0:T(8,128)(2,1)} %param.15) | copy-start | bytes 393220
  274.8 12.2 %all-to-all-start.4 = ((f32[8,1,256]{2,1,0:T(1,128)}), f32[8,1,256]{2,1,0:T(1,128)}, u32[]{:S(2)}, u32[]{:S(2)}) async-start(f32[8,1,256]{2,1,0:T(1,128)} %broadcast_in_dim.13), calls=%async_computation.5 | async-start | bytes 16384 | tf_op jit(solution)/shard_map/all_to_all | solution.py:14
  287.0 12.3 %all-to-all-start.3 = ((f32[8,32,384]{2,1,0:T(8,128)}), f32[8,32,384]{2,1,0:T(8,128)S(1)}, u32[]{:S(2)}, u32[]{:S(2)}) async-start(f32[8,32,384]{2,1,0:T(8,128)} %bitcast.44), calls=%async_computation.4 | async-start | bytes 786432 | tf_op jit(solution)/shard_map/all_to_all | solution.py:30
  291.8 14.2 %copy-start.15 = (f32[64]{0:T(128)S(1)}, f32[64]{0:T(128)}, u32[]{:S(2)}) copy-start(f32[64]{0:T(128)} %get-tuple-element.19) | copy-start | bytes 772
  291.8 153.3 %reduce-scatter.5.cloned.1.call-start = ((), (), s32[]{:S(2)}) async-start(), calls=%async_computation.9 | async-start | bytes 540672 | tf_op jit(solution)/shard_map/reduce_scatter | solution.py:47
  303.0 0.6 copy-start.11
  305.7 10.3 %copy-start.4 = (f32[32,64]{1,0:T(8,128)S(1)}, f32[32,64]{1,0:T(8,128)}, u32[]{:S(2)}) copy-start(f32[32,64]{1,0:T(8,128)} %copy-done.3) | copy-start | bytes 24580
  305.7 10.3 %copy-start.6 = (f32[32,64]{1,0:T(8,128)S(1)}, f32[32,64]{1,0:T(8,128)}, u32[]{:S(2)}) copy-start(f32[32,64]{1,0:T(8,128)} %copy-done.5) | copy-start | bytes 24580
  305.7 10.3 %copy-start.8 = (f32[32,64]{1,0:T(8,128)S(1)}, f32[32,64]{1,0:T(8,128)}, u32[]{:S(2)}) copy-start(f32[32,64]{1,0:T(8,128)} %copy-done.7) | copy-start | bytes 24580
  305.7 10.3 %copy-start.10 = (f32[32,64]{1,0:T(8,128)S(1)}, f32[32,64]{1,0:T(8,128)}, u32[]{:S(2)}) copy-start(f32[32,64]{1,0:T(8,128)} %copy-done.9) | copy-start | bytes 24580
  314.1 2.0 copy-start.12
Sparse Core Ops, SparseCore 0:
  60.8 129.9 reduce-scatter.2
  315.3 129.8 reduce-scatter.4
where the time goes:
time: 537 us; the launch traced here: 536 us
  waiting for transfers between devices  267 us (50%)
  blocking collectives  181 us (34%)
  starting transfers between devices  30.8 us (6%)
  matrix products  21.2 us (4%)
  between operations  15 us (3%)
  local copies, waits for them, and re-layouts  11 us (2%)
  other arithmetic  9.12 us (2%)
    reduce_scatter x2, waiting for transfers between devices, scatter_axes(): nearer = lax.psum_scatter(array, axes[0], scatter_dimension=dim, tiled=True)  254 us
    all_gather x4, blocking collectives, all_blocks(): parts = lax.all_gather(parts, axes[k])  130 us
    unnamed x2, blocking collectives  35 us
    all_to_all x2, starting transfers between devices, sent_to_all(): return lax.all_to_all(copies, axis, split_axis=0, concat_axis=0, tiled=True)  21.2 us
    all_to_all x2, blocking collectives, sent_to_all(): return lax.all_to_all(copies, axis, split_axis=0, concat_axis=0, tiled=True)  15.6 us
    all_to_all x2, waiting for transfers between devices, sent_and_summed(): lax.all_to_all(parts, axis, split_axis=0, concat_axis=0, tiled=True)  12.9 us
    dot_general x12, matrix products, per_device(): jnp.dot(scaled_in, matrix, preferred_element_type=jnp.float32)  11.6 us
  transfers between devices with their start and end apart: 6, of which 4 were waited for; matrix products, arithmetic and copies ran while one was open for 4% of the time, Pallas kernels for 0%

commit v1 on v0

v1 whole, which is shorter than its diff:
```python
import functools

import jax
import jax.numpy as jnp
from jax import lax
from jax.experimental import pallas as pl
from jax.experimental.pallas import tpu as pltpu
from jax.sharding import Mesh
from jax.sharding import PartitionSpec as P

MESH = pl.DeviceIdType.MESH
F32 = jnp.float32
BF16 = jnp.bfloat16
NZ, NY, NX, NC = 32, 4, 4, 2
NDP = NX * NC
D = 4096
HC = 64
SEQ = 32
NT = (((1,), (1,)), ((), ()))
NN = (((1,), (0,)), ((), ()))


def kernel(
    tok_hbm, gain_ref, wr, wk, wv, wd, wa, wg, floor_ref, direct_ref, norm_ref, wo_hbm, st_hbm,
    hid_out, st_out,
    hid, wt, wo, st, st2, psend, precv, osend, oget, ysend, yrecv, zsend, zrecv,
    load_sem, p_ss, p_rs, o_ss, o_rs, y_ss, y_rs, z_ss, z_rs, g_ss, g_rs, h_ss, h_rs, out_sem,
):
    zi, yi = lax.axis_index("z"), lax.axis_index("y")
    xi, ci = lax.axis_index("x"), lax.axis_index("c")
    di = xi * NC + ci

    def dp_peer(k):
        d = lax.rem(di + k, NDP)
        return d, {"x": lax.div(d, NC), "c": lax.rem(d, NC)}

    def y_peer(k):
        p = lax.rem(yi + k, NY)
        return p, {"y": p}

    def z_peer(k):
        p = lax.rem(zi + k, NZ)
        return p, {"z": p}

    def remote(src, dst, ss, rs, dev):
        return pltpu.make_async_remote_copy(
            src_ref=src, dst_ref=dst, send_sem=ss, recv_sem=rs, device_id=dev, device_id_type=MESH
        )

    loads = [pltpu.make_async_copy(tok_hbm, hid.at[0], load_sem.at[0])]
    for l in range(2):
        for p, w in enumerate((wr, wk, wv, wd, wa, wg)):
            loads.append(
                pltpu.make_async_copy(w.at[l], wt.at[l, pl.ds(64 * p, 64)], load_sem.at[1 + 6 * l + p])
            )
    state_loads = [pltpu.make_async_copy(st_hbm.at[l], st.at[l], load_sem.at[13 + l]) for l in range(2)]
    wo_load = pltpu.make_async_copy(wo_hbm, wo, load_sem.at[15])
    for cp in loads[:7]:
        cp.start()
    state_loads[0].start()
    wo_load.start()
    for cp in loads[7:]:
        cp.start()
    state_loads[1].start()

    barrier = pltpu.get_barrier_semaphore()

    def greet_z(k, _):
        pl.semaphore_signal(barrier, inc=1, device_id=z_peer(k)[1], device_id_type=MESH)
        return 0

    lax.fori_loop(1, NZ, greet_z, 0)
    for k in range(1, NDP):
        pl.semaphore_signal(barrier, inc=1, device_id=dp_peer(k)[1], device_id_type=MESH)
    for k in range(1, NY):
        pl.semaphore_signal(barrier, inc=1, device_id=y_peer(k)[1], device_id_type=MESH)

    for l in range(2):
        if l == 0:
            loads[0].wait()
        for cp in loads[1 + 6 * l : 7 + 6 * l]:
            cp.wait()
        hv = hid[l].astype(F32).reshape(NZ, 4, 8, 128)
        sq = None
        xs = []
        for cg in range(4):
            part = hv[:, cg].reshape(256, 128)
            sq = part * part if sq is None else sq + part * part
            xs.append((part * gain_ref[l : l + 1, 128 * cg : 128 * cg + 128]).astype(BF16))
        sq = jnp.sum(sq, axis=1, keepdims=True)
        high = sq.astype(BF16).astype(F32)
        low = sq - high
        lane = lax.broadcasted_iota(jnp.int32, (256, 128), 1)
        tail = jnp.where(lane == 0, high, jnp.where(lane == 1, low, 0.0)).astype(BF16)
        proj = lax.dot_general(
            jnp.concatenate(xs, axis=1), wt[l], NT, preferred_element_type=F32
        ).astype(BF16)
        psend[l, :, :, 0:384] = proj.reshape(NDP, SEQ, 384)
        psend[l, :, :, 384:512] = tail.reshape(NDP, SEQ, 128)
        if l == 0:
            pl.semaphore_wait(barrier, (NZ - 1) + (NDP - 1) + (NY - 1))
        for k in range(1, NDP):
            d, dev = dp_peer(k)
            remote(psend.at[l, d], precv.at[l, di], p_ss.at[l], p_rs.at[l], dev).start()
        total = psend[l, di].astype(F32)
        if l == 0:
            state_loads[0].wait()
        else:
            state_loads[1].wait()
        remote(
            psend.at[l, pl.ds(0, NDP - 1)], precv.at[l, pl.ds(0, NDP - 1)], p_ss.at[l], p_rs.at[l], {"y": lax.rem(yi + 1, NY)}
        ).wait_recv()
        for k in range(1, NDP):
            total = total + precv[l, lax.rem(di + k, NDP)].astype(F32)
        squares = total[:, 384:385] + total[:, 385:386]
        total = total[:, 0:384] * lax.rsqrt(squares * (1.0 / D) + 1e-6)
        r, k_, v, pd, pa, pg = [total[:, 64 * p : 64 * p + 64] for p in range(6)]
        decay = jnp.exp(-0.6065306597126334 * jax.nn.sigmoid(floor_ref[l : l + 1, :] + pd))
        rate = jax.nn.sigmoid(pa)
        gate = jax.nn.sigmoid(pg)
        u = k_ * lax.rsqrt(jnp.sum(k_ * k_, axis=1, keepdims=True) + 1e-6)
        kr = k_ * rate
        ur = u * rate
        dr = decay * r
        row16 = lax.broadcasted_iota(jnp.int32, (16, 64), 0) % 8
        cs, ys = [], []
        for q in range(4):
            rows = slice(8 * q, 8 * q + 8)
            left = jnp.concatenate([u[rows], dr[rows]], axis=0).astype(BF16)
            blk = st[l, rows].reshape(512, 64).astype(BF16)
            res = lax.dot_general(left, blk, NT, preferred_element_type=F32)
            acc = jnp.zeros((16, 64), F32)
            for t in range(8):
                acc = jnp.where(row16 == t, res[:, 64 * t : 64 * t + 64], acc)
            cs.append(acc[0:8])
            ys.append(acc[8:16])
        c = -jnp.concatenate(cs, axis=0)
        y = (
            jnp.concatenate(ys, axis=0)
            + c * jnp.sum(ur * r, axis=1, keepdims=True)
            + v * jnp.sum(kr * r, axis=1, keepdims=True)
        )
        y = y - jnp.mean(y, axis=1, keepdims=True)
        var = jnp.mean(y * y, axis=1, keepdims=True)
        o = y * lax.rsqrt(var + 0.00064) * norm_ref[l : l + 1, :]
        o = o + jnp.sum(r * kr * direct_ref[l : l + 1, :], axis=1, keepdims=True) * v
        o = o * gate
        osend[l] = jnp.concatenate([o, jnp.zeros_like(o)], axis=1).astype(BF16)
        for k in range(1, NDP):
            _, dev = dp_peer(k)
            remote(osend.at[l], oget.at[l, di], o_ss.at[l], o_rs.at[l], dev).start()
        oget[l, di] = osend[l]
        ct = c.T
        vt = v.T

        def update(lo, hi):
            for s in range(lo, hi):
                st2[l, s] = (
                    st[l, s] * decay[s : s + 1, :]
                    + ct[:, s : s + 1] * ur[s : s + 1, :]
                    + vt[:, s : s + 1] * kr[s : s + 1, :]
                )

        if l == 0:
            wo_load.wait()
        remote(
            oget.at[l, pl.ds(0, NDP - 1)], oget.at[l, pl.ds(0, NDP - 1)], o_ss.at[l], o_rs.at[l], {"y": lax.rem(yi + 1, NY)}
        ).wait_recv()
        for k in (2, 1, 3, 0):
            p, dev = y_peer(k)
            rows = oget[l, pl.ds(2 * p, 2)].reshape(64, 128)[:, 0:64]
            share = lax.dot_general(rows, wo[l], NN, preferred_element_type=F32).astype(BF16)
            for rg in range(8):
                for cg in range(4):
                    ysend[l, p, rg * 4 + cg] = share[8 * rg : 8 * rg + 8, 128 * cg : 128 * cg + 128]
            if k:
                remote(ysend.at[l, p], yrecv.at[l, k - 1], y_ss.at[l], y_rs.at[l], dev).start()
        remote(
            yrecv.at[l, pl.ds(0, 3)], yrecv.at[l, pl.ds(0, 3)], y_ss.at[l], y_rs.at[l], {"y": lax.rem(yi + 1, NY)}
        ).wait_recv()
        summed = ysend[l, yi].astype(F32)
        for k in range(3):
            summed = summed + yrecv[l, k].astype(F32)
        zsend[l] = summed.astype(BF16)

        def z_scatter(k, _):
            far = jnp.where(k % 2 == 0, NZ // 2 + k // 2, NZ // 2 - (k + 1) // 2)
            p, dev = z_peer(far)
            remote(zsend.at[l, p], zrecv.at[l, zi], z_ss.at[l], z_rs.at[l], dev).start()
            return 0

        lax.fori_loop(0, NZ - 1, z_scatter, 0)
        zrecv[l, zi] = zsend[l, zi]
        update(0, SEQ)
        state_store = pltpu.make_async_copy(st2.at[l], st_out.at[l], out_sem.at[l])
        state_store.start()
        remote(
            zrecv.at[l, pl.ds(0, NZ - 1)], zrecv.at[l, pl.ds(0, NZ - 1)], z_ss.at[l], z_rs.at[l], {"z": lax.rem(zi + 1, NZ)}
        ).wait_recv()
        mine = jnp.sum(zrecv[l].astype(F32), axis=0) + hid[l, yi, zi].astype(F32)
        hid[l + 1, yi, zi] = mine.astype(BF16)

        def z_gather(k, _):
            far = jnp.where(k % 2 == 0, NZ // 2 + k // 2, NZ // 2 - (k + 1) // 2)
            _, dev = z_peer(far)
            own = hid.at[l + 1, yi, zi]
            remote(own, own, g_ss.at[l], g_rs.at[l], dev).start()
            return 0

        lax.fori_loop(0, NZ - 1, z_gather, 0)
        some = hid.at[l + 1, yi, pl.ds(0, NZ - 1)]
        remote(some, some, g_ss.at[l], g_rs.at[l], {"z": lax.rem(zi + 1, NZ)}).wait_recv()
        for k in (2, 1, 3):
            _, dev = y_peer(k)
            own = hid.at[l + 1, yi]
            remote(own, own, h_ss.at[l], h_rs.at[l], dev).start()
        three = hid.at[l + 1, pl.ds(0, 3)]
        remote(three, three, h_ss.at[l], h_rs.at[l], {"y": lax.rem(yi + 1, NY)}).wait_recv()

    hid_store = pltpu.make_async_copy(hid.at[2], hid_out, out_sem.at[2])
    hid_store.start()
    for l in range(2):
        near = {"y": lax.rem(yi + 1, NY)}
        for buf, count, ss, rs in (
            (psend.at[l, pl.ds(0, NDP - 1)], None, p_ss, p_rs),
            (oget.at[l, pl.ds(0, NDP - 1)], None, o_ss, o_rs),
            (yrecv.at[l, pl.ds(0, 3)], None, y_ss, y_rs),
            (zsend.at[l, pl.ds(0, NZ - 1)], None, z_ss, z_rs),
            (zsend.at[l, pl.ds(0, NZ - 1)], None, g_ss, g_rs),
            (yrecv.at[l, pl.ds(0, 3)], None, h_ss, h_rs),
        ):
            remote(buf, buf, ss.at[l], rs.at[l], near).wait_send()
        pltpu.make_async_copy(st2.at[l], st_out.at[l], out_sem.at[l]).wait()
    hid_store.wait()


def per_device(
    incoming_token, input_norm_gain, receptance_weight, key_weight, value_weight, decay_weight,
    learning_rate_weight, gate_weight, channel_decay_floor, direct_token_weight, head_norm_gain,
    output_weight, incoming_state,
):
    tiles = incoming_token.reshape(NZ, 8, 4, 128).transpose(0, 2, 1, 3).reshape(NY, NZ, 8, 128)
    weights = [
        jnp.swapaxes(w, 1, 2)
        for w in (
            receptance_weight, key_weight, value_weight, decay_weight, learning_rate_weight, gate_weight,
        )
    ]
    state = incoming_state.reshape(2, SEQ, HC, HC)
    anywhere = pl.BlockSpec(memory_space=pl.ANY)
    vmem = pl.BlockSpec(memory_space=pltpu.VMEM)
    dma = pltpu.SemaphoreType.DMA
    hidden, new_state = pl.pallas_call(
        kernel,
        out_shape=(
            jax.ShapeDtypeStruct((NY, NZ, 8, 128), BF16),
            jax.ShapeDtypeStruct((2, SEQ, HC, HC), F32),
        ),
        in_specs=[anywhere, vmem] + [anywhere] * 6 + [vmem] * 3 + [anywhere] * 2,
        out_specs=(anywhere, anywhere),
        scratch_shapes=[
            pltpu.VMEM((3, NY, NZ, 8, 128), BF16),
            pltpu.VMEM((2, 384, 512), BF16),
            pltpu.VMEM((2, HC, 512), BF16),
            pltpu.VMEM((2, SEQ, HC, HC), F32),
            pltpu.VMEM((2, SEQ, HC, HC), F32),
            pltpu.VMEM((2, NDP, SEQ, 512), BF16),
            pltpu.VMEM((2, NDP, SEQ, 512), BF16),
            pltpu.VMEM((2, SEQ, 128), BF16),
            pltpu.VMEM((2, NDP, SEQ, 128), BF16),
            pltpu.VMEM((2, NY, NZ, 8, 128), BF16),
            pltpu.VMEM((2, 3, NZ, 8, 128), BF16),
            pltpu.VMEM((2, NZ, 8, 128), BF16),
            pltpu.VMEM((2, NZ, 8, 128), BF16),
            dma((16,)),
            *[dma((2,)) for _ in range(12)],
            dma((3,)),
        ],
        compiler_params=pltpu.CompilerParams(
            collective_id=0, has_side_effects=True, vmem_limit_bytes=48 * 1024 * 1024
        ),
        name="decode_step",
    )(
        tiles, input_norm_gain, *weights, channel_decay_floor, direct_token_weight, head_norm_gain,
        output_weight, state,
    )
    hidden = hidden.reshape(NZ, 4, 8, 128).transpose(0, 2, 1, 3).reshape(256, 512)
    return (hidden, new_state.reshape(2, SEQ, 1, HC, HC))


def solution(mesh):
    finer = Mesh(mesh.devices.reshape(NZ, NY, NX, NC), ("z", "y", "x", "c"))
    tp, dp = ("z", "y"), ("x", "c")
    w = P(None, dp, tp)
    return jax.shard_map(
        per_device,
        mesh=finer,
        in_specs=(
            P(None, dp), P(None, dp), w, w, w, w, w, w, P(None, tp), P(None, tp), P(None, tp),
            P(None, tp, dp), P(None, dp, tp, None, None),
        ),
        out_specs=(P(None, dp), P(None, dp, tp, None, None)),
        check_vma=False,
    )
```

time: 537 us -> 133 us (0.25)
  the two profiles are of different devices: /device:TPU:2 before, /device:TPU:8 now
where the time goes in v1:
time: 133 us
  Pallas kernels  119 us (89%)
  local copies, waits for them, and re-layouts  13.6 us (10%)
    pallas_call x1, Pallas kernels, per_device(): pl.pallas_call(kernel, out_shape=(jax.ShapeDtypeStruct((NY, NZ, 8, 128),...  119 us
    unnamed x28, local copies, waits for them, and re-layouts  13.6 us

profile of v1, /device:TPU:8, one launch (start us, length us, event | category | flops | bytes accessed | tf_op | source)
XLA Modules:
  0.0 132.9 jit_solution(850687121276203540)
XLA Ops:
  0.6 0.0 copy-start
  0.6 1.6 %copy-done = f32[2,32,1,64,64]{4,3,2,1,0:T(8,128)S(1)} copy-done((f32[2,32,1,64,64]{4,3,2,1,0:T(8,128)S(1)}, f32[2,32,1,64,64]{4,3,2,1,0:T(8,128)}, u32[]{:S(2)}) %copy-start) | copy-done | bytes 1048600
  2.2 0.0 copy-start.1
  2.2 0.9 copy-done.1
  3.2 0.0 copy-start.2
  3.2 0.9 copy-done.2
  4.1 0.0 copy-start.3
  4.1 0.9 copy-done.3
  5.0 0.0 copy-start.4
  5.0 0.9 copy-done.4
  5.9 0.0 copy-start.5
  5.9 0.9 copy-done.5
  6.8 0.0 copy-start.6
  6.8 0.9 copy-done.6
  7.7 0.0 copy-start.7
  7.7 0.9 copy-done.7
  8.6 0.0 copy-start.8
  8.6 0.9 copy-done.8
  9.5 0.0 copy-start.9
  9.5 0.7 copy-done.9
  10.2 0.0 copy-start.10
  10.2 0.7 copy-done.10
  10.9 0.0 copy-start.11
  10.9 0.7 copy-done.11
  11.6 0.0 copy-start.12
  11.6 0.7 copy-done.12
  12.2 118.6 %decode_step.1 = (bf16[4,32,8,128]{3,2,1,0:T(8,128)(2,1)S(1)}, f32[2,32,64,64]{3,2,1,0:T(8,128)S(1)}) custom-call(bf16[4,32,8,128]{3,2,1,0:T(8,128)(2,1)S(1)} %bitcast.23, f32[2,512]{1,0:T(2,128)S(1)} %copy-done.9, bf16[2,64,512]{2,1,0:T(8,128)(2,1)S(1)} %bitcast.24, bf16[2,64,512]{2,1,0:T(8,128)(2,1)S(1)} %bitcast.25, bf16[2,64,512]{2,1,0:T(8,128)(2,1)S(1)} %bitcast.26, ...), custom_call_target="tpu_custom_call" | custom-call | tf_op jit(solution)/shard_map/decode_step/pallas_call | solution.py:253
  130.8 0.7 copy.18
  131.5 1.3 copy.19
Async XLA Ops:
  0.6 1.6 %copy-start = (f32[2,32,1,64,64]{4,3,2,1,0:T(8,128)S(1)}, f32[2,32,1,64,64]{4,3,2,1,0:T(8,128)}, u32[]{:S(2)}) copy-start(f32[2,32,1,64,64]{4,3,2,1,0:T(8,128)} %param.25) | copy-start | bytes 3145732
  2.2 0.9 copy-start.1
  3.2 0.9 copy-start.2
  4.1 0.9 copy-start.3
  5.0 0.9 copy-start.4
  5.9 0.9 copy-start.5
  6.8 0.9 copy-start.6
  7.7 0.9 copy-start.7
  8.6 0.9 copy-start.8
  9.5 0.7 copy-start.9
  10.2 0.7 copy-start.10
  10.9 0.7 copy-start.11
  11.6 0.7 copy-start.12

commit v2 on v1

--- a/solution.py
+++ b/solution.py
@@ -18,13 +18,14 @@
 SEQ = 32
 NT = (((1,), (1,)), ((), ()))
 NN = (((1,), (0,)), ((), ()))
+GROUPS = ((0, 7), (7, 15), (15, 31))
 
 
 def kernel(
-    tok_hbm, gain_ref, wr, wk, wv, wd, wa, wg, floor_ref, direct_ref, norm_ref, wo_hbm, st_hbm,
+    tok_hbm, gain_hbm, wr, wk, wv, wd, wa, wg, floor_hbm, direct_hbm, norm_hbm, wo_hbm, st_hbm,
     hid_out, st_out,
-    hid, wt, wo, st, st2, psend, precv, osend, oget, ysend, yrecv, zsend, zrecv,
-    load_sem, p_ss, p_rs, o_ss, o_rs, y_ss, y_rs, z_ss, z_rs, g_ss, g_rs, h_ss, h_rs, out_sem,
+    hid, gain_ref, floor_ref, direct_ref, norm_ref, wt, wo, st, psend, precv, osend, oget, ysend, yrecv, zsend, zrecv,
+    load_sem, p_ss, p_rs, o_ss, o_rs, y_ss, y_rs, z_ss, z_rs, g_ss, g_rs, h_ss, h_rs, within8, within16,
 ):
     zi, yi = lax.axis_index("z"), lax.axis_index("y")
     xi, ci = lax.axis_index("x"), lax.axis_index("c")
@@ -46,6 +47,14 @@
         return pltpu.make_async_remote_copy(
             src_ref=src, dst_ref=dst, send_sem=ss, recv_sem=rs, device_id=dev, device_id_type=MESH
         )
+
+    def far_first(k):
+        return jnp.where(k % 2 == 0, NZ // 2 + k // 2, NZ // 2 - (k + 1) // 2)
+
+    def y_copy(l, k, h):
+        p, dev = y_peer(k)
+        part = pl.ds(16 * h, 16)
+        return remote(ysend.at[l, p, part], yrecv.at[l, k - 1, part], y_ss.at[l], y_rs.at[l, h], dev)
 
     loads = [pltpu.make_async_copy(tok_hbm, hid.at[0], load_sem.at[0])]
     for l in range(2):
@@ -55,7 +64,16 @@
             )
     state_loads = [pltpu.make_async_copy(st_hbm.at[l], st.at[l], load_sem.at[13 + l]) for l in range(2)]
     wo_load = pltpu.make_async_copy(wo_hbm, wo, load_sem.at[15])
-    for cp in loads[:7]:
+    smalls = [
+        pltpu.make_async_copy(a, b, load_sem.at[16 + i])
+        for i, (a, b) in enumerate(
+            ((gain_hbm, gain_ref), (floor_hbm, floor_ref), (direct_hbm, direct_ref), (norm_hbm, norm_ref))
+        )
+    ]
+    loads[0].start()
+    for cp in smalls:
+        cp.start()
+    for cp in loads[1:7]:
         cp.start()
     state_loads[0].start()
     wo_load.start()
@@ -65,11 +83,8 @@
 
     barrier = pltpu.get_barrier_semaphore()
 
-    def greet_z(k, _):
+    for k in (1, 2, 3, 4, NZ - 4, NZ - 3, NZ - 2, NZ - 1):
         pl.semaphore_signal(barrier, inc=1, device_id=z_peer(k)[1], device_id_type=MESH)
-        return 0
-
-    lax.fori_loop(1, NZ, greet_z, 0)
     for k in range(1, NDP):
         pl.semaphore_signal(barrier, inc=1, device_id=dp_peer(k)[1], device_id_type=MESH)
     for k in range(1, NY):
@@ -78,6 +93,8 @@
     for l in range(2):
         if l == 0:
             loads[0].wait()
+            for cp in smalls:
+                cp.wait()
         for cp in loads[1 + 6 * l : 7 + 6 * l]:
             cp.wait()
         hv = hid[l].astype(F32).reshape(NZ, 4, 8, 128)
@@ -98,18 +115,28 @@
         psend[l, :, :, 0:384] = proj.reshape(NDP, SEQ, 384)
         psend[l, :, :, 384:512] = tail.reshape(NDP, SEQ, 128)
         if l == 0:
-            pl.semaphore_wait(barrier, (NZ - 1) + (NDP - 1) + (NY - 1))
-        for k in range(1, NDP):
+            with jax.named_scope("w_bar"):
+                pl.semaphore_wait(barrier, 8 + (NDP - 1) + (NY - 1))
+            for k in (4, NZ - 4):
+                pl.semaphore_signal(within8, inc=1, device_id=z_peer(k)[1], device_id_type=MESH)
+        for k in (4, 3, 5, 2, 6, 1, 7):
             d, dev = dp_peer(k)
             remote(psend.at[l, d], precv.at[l, di], p_ss.at[l], p_rs.at[l], dev).start()
         total = psend[l, di].astype(F32)
         if l == 0:
-            state_loads[0].wait()
+            with jax.named_scope("w_st"):
+                state_loads[0].wait()
         else:
-            state_loads[1].wait()
-        remote(
-            psend.at[l, pl.ds(0, NDP - 1)], precv.at[l, pl.ds(0, NDP - 1)], p_ss.at[l], p_rs.at[l], {"y": lax.rem(yi + 1, NY)}
-        ).wait_recv()
+            with jax.named_scope("w_st"):
+                state_loads[1].wait()
+        with jax.named_scope("w_p"):
+            remote(
+                psend.at[l, pl.ds(0, NDP - 1)], precv.at[l, pl.ds(0, NDP - 1)], p_ss.at[l], p_rs.at[l], {"y": lax.rem(yi + 1, NY)}
+            ).wait_recv()
+        if l == 0:
+            pl.semaphore_wait(within8, 2)
+            for k in (8, NZ - 8):
+                pl.semaphore_signal(within16, inc=1, device_id=z_peer(k)[1], device_id_type=MESH)
         for k in range(1, NDP):
             total = total + precv[l, lax.rem(di + k, NDP)].astype(F32)
         squares = total[:, 384:385] + total[:, 385:386]
@@ -146,7 +173,7 @@
         o = o + jnp.sum(r * kr * direct_ref[l : l + 1, :], axis=1, keepdims=True) * v
         o = o * gate
         osend[l] = jnp.concatenate([o, jnp.zeros_like(o)], axis=1).astype(BF16)
-        for k in range(1, NDP):
+        for k in (4, 3, 5, 2, 6, 1, 7):
             _, dev = dp_peer(k)
             remote(osend.at[l], oget.at[l, di], o_ss.at[l], o_rs.at[l], dev).start()
         oget[l, di] = osend[l]
@@ -155,7 +182,7 @@
 
         def update(lo, hi):
             for s in range(lo, hi):
-                st2[l, s] = (
+                st_out[l, s] = (
                     st[l, s] * decay[s : s + 1, :]
                     + ct[:, s : s + 1] * ur[s : s + 1, :]
                     + vt[:, s : s + 1] * kr[s : s + 1, :]
@@ -163,75 +190,97 @@
 
         if l == 0:
             wo_load.wait()
-        remote(
-            oget.at[l, pl.ds(0, NDP - 1)], oget.at[l, pl.ds(0, NDP - 1)], o_ss.at[l], o_rs.at[l], {"y": lax.rem(yi + 1, NY)}
-        ).wait_recv()
+        with jax.named_scope("w_o"):
+            remote(
+                oget.at[l, pl.ds(0, NDP - 1)], oget.at[l, pl.ds(0, NDP - 1)], o_ss.at[l], o_rs.at[l], {"y": lax.rem(yi + 1, NY)}
+            ).wait_recv()
         for k in (2, 1, 3, 0):
             p, dev = y_peer(k)
             rows = oget[l, pl.ds(2 * p, 2)].reshape(64, 128)[:, 0:64]
             share = lax.dot_general(rows, wo[l], NN, preferred_element_type=F32).astype(BF16)
             for rg in range(8):
                 for cg in range(4):
-                    ysend[l, p, rg * 4 + cg] = share[8 * rg : 8 * rg + 8, 128 * cg : 128 * cg + 128]
+                    j = lax.rem(rg * 4 + cg + (NZ - 8) + NZ - zi, NZ)
+                    ysend[l, p, j] = share[8 * rg : 8 * rg + 8, 128 * cg : 128 * cg + 128]
             if k:
-                remote(ysend.at[l, p], yrecv.at[l, k - 1], y_ss.at[l], y_rs.at[l], dev).start()
-        remote(
-            yrecv.at[l, pl.ds(0, 3)], yrecv.at[l, pl.ds(0, 3)], y_ss.at[l], y_rs.at[l], {"y": lax.rem(yi + 1, NY)}
-        ).wait_recv()
-        summed = ysend[l, yi].astype(F32)
-        for k in range(3):
-            summed = summed + yrecv[l, k].astype(F32)
-        zsend[l] = summed.astype(BF16)
-
-        def z_scatter(k, _):
-            far = jnp.where(k % 2 == 0, NZ // 2 + k // 2, NZ // 2 - (k + 1) // 2)
-            p, dev = z_peer(far)
-            remote(zsend.at[l, p], zrecv.at[l, zi], z_ss.at[l], z_rs.at[l], dev).start()
-            return 0
-
-        lax.fori_loop(0, NZ - 1, z_scatter, 0)
-        zrecv[l, zi] = zsend[l, zi]
-        update(0, SEQ)
-        state_store = pltpu.make_async_copy(st2.at[l], st_out.at[l], out_sem.at[l])
-        state_store.start()
-        remote(
-            zrecv.at[l, pl.ds(0, NZ - 1)], zrecv.at[l, pl.ds(0, NZ - 1)], z_ss.at[l], z_rs.at[l], {"z": lax.rem(zi + 1, NZ)}
-        ).wait_recv()
+                y_copy(l, k, 0).start()
+        for k in (2, 1, 3):
+            y_copy(l, k, 1).start()
+        if l == 0:
+            with jax.named_scope("w_16"):
+                pl.semaphore_wait(within16, 2)
+        for h in range(2):
+            part = pl.ds(16 * h, 16)
+            with jax.named_scope("w_y"):
+                some = yrecv.at[l, pl.ds(0, 3), part]
+                remote(some, some, y_ss.at[l], y_rs.at[l, h], y_peer(1)[1]).wait_recv()
+            summed = ysend[l, yi, part].astype(F32)
+            for k in range(3):
+                summed = summed + yrecv[l, k, part].astype(F32)
+            zsend[l, part] = summed.astype(BF16)
+
+            def z_scatter(k, _):
+                off = far_first(k)
+                _, dev = z_peer(off)
+                src = zsend.at[l, lax.rem(off + (NZ - 8), NZ)]
+                remote(src, zrecv.at[l, zi], z_ss.at[l], z_rs.at[l], dev).start()
+                return 0
+
+            with jax.named_scope("zsend"):
+                lax.fori_loop(16 * h, 16 + 15 * h, z_scatter, 0)
+        zrecv[l, zi] = zsend[l, NZ - 8]
+        with jax.named_scope("upd"):
+            update(0, SEQ)
+        with jax.named_scope("w_z"):
+            some = zrecv.at[l, pl.ds(0, NZ - 1)]
+            remote(some, some, z_ss.at[l], z_rs.at[l], z_peer(1)[1]).wait_recv()
         mine = jnp.sum(zrecv[l].astype(F32), axis=0) + hid[l, yi, zi].astype(F32)
         hid[l + 1, yi, zi] = mine.astype(BF16)
 
-        def z_gather(k, _):
-            far = jnp.where(k % 2 == 0, NZ // 2 + k // 2, NZ // 2 - (k + 1) // 2)
-            _, dev = z_peer(far)
-            own = hid.at[l + 1, yi, zi]
-            remote(own, own, g_ss.at[l], g_rs.at[l], dev).start()
-            return 0
-
-        lax.fori_loop(0, NZ - 1, z_gather, 0)
-        some = hid.at[l + 1, yi, pl.ds(0, NZ - 1)]
-        remote(some, some, g_ss.at[l], g_rs.at[l], {"z": lax.rem(zi + 1, NZ)}).wait_recv()
-        for k in (2, 1, 3):
-            _, dev = y_peer(k)
-            own = hid.at[l + 1, yi]
-            remote(own, own, h_ss.at[l], h_rs.at[l], dev).start()
+        own = hid.at[l + 1, yi, zi]
+        for g, (lo, hi) in enumerate(GROUPS):
+
+            def z_gather(k, _):
+                _, dev = z_peer(far_first(k))
+                remote(own, own, g_ss.at[l], g_rs.at[l, g], dev).start()
+                return 0
+
+            with jax.named_scope("zsend"):
+                lax.fori_loop(lo, hi, z_gather, 0)
+
+        def forward(chunk):
+            for k in (2, 1, 3):
+                remote(chunk, chunk, h_ss.at[l], h_rs.at[l], y_peer(k)[1]).start()
+
+        forward(own)
+        for g in range(len(GROUPS) - 1, -1, -1):
+            lo, hi = GROUPS[g]
+            with jax.named_scope("w_g"):
+                some = zsend.at[l, pl.ds(0, hi - lo)]
+                remote(some, some, g_ss.at[l], g_rs.at[l, g], z_peer(1)[1]).wait_recv()
+
+            def onward(k, _):
+                forward(hid.at[l + 1, yi, z_peer(far_first(k))[0]])
+                return 0
+
+            with jax.named_scope("fwd"):
+                lax.fori_loop(lo, hi, onward, 0)
         three = hid.at[l + 1, pl.ds(0, 3)]
-        remote(three, three, h_ss.at[l], h_rs.at[l], {"y": lax.rem(yi + 1, NY)}).wait_recv()
-
-    hid_store = pltpu.make_async_copy(hid.at[2], hid_out, out_sem.at[2])
-    hid_store.start()
+        with jax.named_scope("w_h"):
+            remote(three, three, h_ss.at[l], h_rs.at[l], {"y": lax.rem(yi + 1, NY)}).wait_recv()
+
+    hid_out[...] = hid[2]
     for l in range(2):
         near = {"y": lax.rem(yi + 1, NY)}
-        for buf, count, ss, rs in (
-            (psend.at[l, pl.ds(0, NDP - 1)], None, p_ss, p_rs),
-            (oget.at[l, pl.ds(0, NDP - 1)], None, o_ss, o_rs),
-            (yrecv.at[l, pl.ds(0, 3)], None, y_ss, y_rs),
-            (zsend.at[l, pl.ds(0, NZ - 1)], None, z_ss, z_rs),
-            (zsend.at[l, pl.ds(0, NZ - 1)], None, g_ss, g_rs),
-            (yrecv.at[l, pl.ds(0, 3)], None, h_ss, h_rs),
+        for buf, ss in (
+            (psend.at[l, pl.ds(0, NDP - 1)], p_ss),
+            (oget.at[l, pl.ds(0, NDP - 1)], o_ss),
+            (yrecv.at[l, pl.ds(0, 3)], y_ss),
+            (zsend.at[l, pl.ds(0, NZ - 1)], z_ss),
+            (zsend.at[l, pl.ds(0, NZ - 1)], g_ss),
+            (yrecv.at[l, pl.ds(0, 3)], h_ss),
         ):
-            remote(buf, buf, ss.at[l], rs.at[l], near).wait_send()
-        pltpu.make_async_copy(st2.at[l], st_out.at[l], out_sem.at[l]).wait()
-    hid_store.wait()
+            remote(buf, buf, ss.at[l], p_rs.at[l], near).wait_send()
 
 
 def per_device(
@@ -253,16 +302,17 @@
     hidden, new_state = pl.pallas_call(
         kernel,
         out_shape=(
-            jax.ShapeDtypeStruct((NY, NZ, 8, 128), BF16),
-            jax.ShapeDtypeStruct((2, SEQ, HC, HC), F32),
+            pltpu.VMEM((NY, NZ, 8, 128), BF16),
+            pltpu.VMEM((2, SEQ, HC, HC), F32),
         ),
-        in_specs=[anywhere, vmem] + [anywhere] * 6 + [vmem] * 3 + [anywhere] * 2,
-        out_specs=(anywhere, anywhere),
+        in_specs=[anywhere] * 13,
+        out_specs=(vmem, vmem),
         scratch_shapes=[
             pltpu.VMEM((3, NY, NZ, 8, 128), BF16),
+            pltpu.VMEM((2, 512), F32),
+            *[pltpu.VMEM((2, HC), F32) for _ in range(3)],
             pltpu.VMEM((2, 384, 512), BF16),
             pltpu.VMEM((2, HC, 512), BF16),
-            pltpu.VMEM((2, SEQ, HC, HC), F32),
             pltpu.VMEM((2, SEQ, HC, HC), F32),
             pltpu.VMEM((2, NDP, SEQ, 512), BF16),
             pltpu.VMEM((2, NDP, SEQ, 512), BF16),
@@ -272,12 +322,17 @@
             pltpu.VMEM((2, 3, NZ, 8, 128), BF16),
             pltpu.VMEM((2, NZ, 8, 128), BF16),
             pltpu.VMEM((2, NZ, 8, 128), BF16),
-            dma((16,)),
-            *[dma((2,)) for _ in range(12)],
-            dma((3,)),
+            dma((20,)),
+            *[dma((2,)) for _ in range(5)],
+            dma((2, 2)),
+            *[dma((2,)) for _ in range(3)],
+            dma((2, len(GROUPS))),
+            *[dma((2,)) for _ in range(2)],
+            pltpu.SemaphoreType.REGULAR,
+            pltpu.SemaphoreType.REGULAR,
         ],
         compiler_params=pltpu.CompilerParams(
-            collective_id=0, has_side_effects=True, vmem_limit_bytes=48 * 1024 * 1024
+            collective_id=0, has_side_effects=True, vmem_limit_bytes=60 * 1024 * 1024
         ),
         name="decode_step",
     )(

time: 133 us -> 107 us (0.80)
  Pallas kernels: 119 us -> 105 us
  local copies, waits for them, and re-layouts: 13.6 us -> 2.02 us
    pallas_call x1, Pallas kernels: 119 us -> 105 us  [per_device(): pl.pallas_call(kernel, out_shape=(pltpu.VMEM((NY, NZ, 8, 128), BF16), plt...]
    unnamed x28 -> x2, local copies, waits for them, and re-layouts: 13.6 us -> 2.02 us
where the time goes in v2:
time: 107 us
  Pallas kernels  105 us (98%)
  local copies, waits for them, and re-layouts  2.02 us (2%)
    pallas_call x1, Pallas kernels, per_device(): pl.pallas_call(kernel, out_shape=(pltpu.VMEM((NY, NZ, 8, 128), BF16), plt...  105 us

profile of v2, /device:TPU:8, one launch (start us, length us, event | category | flops | bytes accessed | tf_op | source)
XLA Modules:
  0.0 107.3 jit_solution(17942387008888316444)
XLA Ops:
  0.6 104.7 %decode_step.1 = (bf16[4,32,8,128]{3,2,1,0:T(8,128)(2,1)S(1)}, f32[2,32,64,64]{3,2,1,0:T(8,128)S(1)}) custom-call(bf16[4,32,8,128]{3,2,1,0:T(8,128)(2,1)} %bitcast.23, f32[2,512]{1,0:T(2,128)} %gain_hbm.1, bf16[2,64,512]{2,1,0:T(8,128)(2,1)} %bitcast.24, bf16[2,64,512]{2,1,0:T(8,128)(2,1)} %bitcast.25, bf16[2,64,512]{2,1,0:T(8,128)(2,1)} %bitcast.26, ...), custom_call_target="tpu_custom_call" | custom-call | tf_op jit(solution)/shard_map/decode_step/pallas_call | solution.py:302
  105.3 0.7 copy.18
  106.0 1.3 %copy.19 = f32[2,32,1,64,64]{4,3,2,1,0:T(8,128)} copy(f32[2,32,1,64,64]{4,3,2,1,0:T(8,128)S(1)} %bitcast.20) | data formatting | bytes 2097152

commit v3 on v2

v3 whole, which is shorter than its diff:
```python
import functools

import jax
import jax.numpy as jnp
from jax import lax
from jax.experimental import pallas as pl
from jax.experimental.pallas import tpu as pltpu
from jax.sharding import Mesh
from jax.sharding import PartitionSpec as P

MESH = pl.DeviceIdType.MESH
F32 = jnp.float32
BF16 = jnp.bfloat16
NZ, NY, NX, NC = 32, 4, 4, 2
NDP = NX * NC
D = 4096
HC = 64
SEQ = 32
NT = (((1,), (1,)), ((), ()))
NN = (((1,), (0,)), ((), ()))
GROUPS = ((0, 3), (3, 7), (7, 11), (11, 15))
DIRECT = 0


def kernel(
    tok_hbm, gain_hbm, wr, wk, wv, wd, wa, wg, floor_hbm, direct_hbm, norm_hbm, wo_hbm, st_hbm,
    hid_out, st_out,
    hid, gain_ref, floor_ref, direct_ref, norm_ref, wt, wo, st, stb, tsend, trecv, psend, precv, osend, oget, zsend, zrecv,
    load_sem, t_ss, t_rs, p_ss, p_rs, o_ss, o_rs, w_ss, w_rs, z_ss, z_rs, g_ss, g_rs, h_ss, h_rs, within8, within16,
):
    zi, yi = lax.axis_index("z"), lax.axis_index("y")
    xi, ci = lax.axis_index("x"), lax.axis_index("c")
    di = xi * NC + ci

    def dp_peer(k):
        d = lax.rem(di + k, NDP)
        return d, {"x": lax.div(d, NC), "c": lax.rem(d, NC)}

    def y_peer(k):
        p = lax.rem(yi + k, NY)
        return p, {"y": p}

    def z_peer(k):
        p = lax.rem(zi + k, NZ)
        return p, {"z": p}

    def remote(src, dst, ss, rs, dev):
        return pltpu.make_async_remote_copy(
            src_ref=src, dst_ref=dst, send_sem=ss, recv_sem=rs, device_id=dev, device_id_type=MESH
        )

    def far_first(k):
        return jnp.where(k % 2 == 0, NZ // 2 + k // 2, NZ // 2 - (k + 1) // 2)

    def near_off(k):
        return jnp.where(k % 2 == 0, NZ - 8 + k // 2, 8 - (k + 1) // 2)

    def o_count(l, wait):
        @pl.when(yi != xi)
        def _():
            wait(oget.at[l])

        @pl.when(yi == xi)
        def _():
            wait(oget.at[l, pl.ds(0, NDP - 1)])

    order = []
    for q in range(16):
        apart = lax.rem(q + NZ - zi, 16)
        order.append(jnp.where(apart < 8, 2 * apart, 31 - 2 * apart))

    barrier = pltpu.get_barrier_semaphore()

    for k in (1, 2, 3, 4, NZ - 4, NZ - 3, NZ - 2, NZ - 1):
        pl.semaphore_signal(barrier, inc=1, device_id=z_peer(k)[1], device_id_type=MESH)
    for k in range(1, NDP):
        pl.semaphore_signal(barrier, inc=1, device_id=dp_peer(k)[1], device_id_type=MESH)
    for k in range(1, NY):
        pl.semaphore_signal(barrier, inc=1, device_id=y_peer(k)[1], device_id_type=MESH)

    loads = [pltpu.make_async_copy(tok_hbm, hid.at[0], load_sem.at[0])]
    for l in range(2):
        for p, w in enumerate((wr, wk, wv, wd, wa, wg)):
            loads.append(
                pltpu.make_async_copy(w.at[l], wt.at[l, pl.ds(64 * p, 64)], load_sem.at[1 + 6 * l + p])
            )
    state_loads = [pltpu.make_async_copy(st_hbm.at[l], st.at[l], load_sem.at[13 + l]) for l in range(2)]
    wo_loads = [pltpu.make_async_copy(wo_hbm.at[l], wo.at[l, yi], load_sem.at[15 + 5 * l]) for l in range(2)]
    smalls = [
        pltpu.make_async_copy(a, b, load_sem.at[16 + i])
        for i, (a, b) in enumerate(
            ((gain_hbm, gain_ref), (floor_hbm, floor_ref), (direct_hbm, direct_ref), (norm_hbm, norm_ref))
        )
    ]
    loads[0].start()
    for cp in smalls:
        cp.start()
    for cp in loads[1:7]:
        cp.start()
    state_loads[0].start()
    wo_loads[0].start()
    for cp in loads[7:]:
        cp.start()
    state_loads[1].start()
    wo_loads[1].start()

    for l in range(2):
        if l == 0:
            loads[0].wait()
            for cp in smalls:
                cp.wait()
        for cp in loads[1 + 6 * l : 7 + 6 * l]:
            cp.wait()
        hv = hid[l].astype(F32).reshape(NZ, 4, 8, 128)
        sq = None
        xs = []
        for cg in range(4):
            part = hv[:, cg].reshape(256, 128)
            sq = part * part if sq is None else sq + part * part
            xs.append((part * gain_ref[l : l + 1, 128 * cg : 128 * cg + 128]).astype(BF16))
        high = sq.astype(BF16)
        ones = jnp.ones((8, 128), BF16)
        sums = lax.dot_general(ones, high, NT, preferred_element_type=F32) + lax.dot_general(
            ones, (sq - high.astype(F32)).astype(BF16), NT, preferred_element_type=F32
        )
        high = sums.astype(BF16).astype(F32)
        sums = jnp.where(lax.broadcasted_iota(jnp.int32, (8, 256), 0) == 0, high, sums - high).astype(BF16)
        tsend[l, 0] = sums[:, 0:128]
        tsend[l, 1] = sums[:, 128:256]
        proj = lax.dot_general(
            jnp.concatenate(xs, axis=1), wt[l], NT, preferred_element_type=F32
        ).astype(BF16)
        psend[l] = proj.reshape(NDP, SEQ, 384)
        if l == 0:
            with jax.named_scope("w_bar"):
                pl.semaphore_wait(barrier, 8 + (NDP - 1) + (NY - 1))
            for k in (4, NZ - 4):
                pl.semaphore_signal(within8, inc=1, device_id=z_peer(k)[1], device_id_type=MESH)
        for k in (4, 3, 5, 2, 6, 1, 7):
            d, dev = dp_peer(k)
            remote(tsend.at[l, lax.div(d, 4)], trecv.at[l, di], t_ss.at[l], t_rs.at[l], dev).start()
        for k in (4, 3, 5, 2, 6, 1, 7):
            d, dev = dp_peer(k)
            remote(psend.at[l, d], precv.at[l, di], p_ss.at[l], p_rs.at[l], dev).start()
        if l == 0:
            wo_loads[0].wait()
            for k in (2, 1, 3):
                remote(wo.at[0, yi], wo.at[0, yi], w_ss.at[0], w_rs.at[0], y_peer(k)[1]).start()
        with jax.named_scope("w_st"):
            state_loads[l].wait()
        stb[...] = st[l].reshape(SEQ * HC, HC).astype(BF16)
        if l == 0:
            with jax.named_scope("w_8"):
                pl.semaphore_wait(within8, 2)
            for k in (8, NZ - 8):
                pl.semaphore_signal(within16, inc=1, device_id=z_peer(k)[1], device_id_type=MESH)
        total = psend[l, di].astype(F32)
        with jax.named_scope("w_p"):
            remote(
                psend.at[l, pl.ds(0, NDP - 1)], precv.at[l, pl.ds(0, NDP - 1)], p_ss.at[l], p_rs.at[l], {"y": lax.rem(yi + 1, NY)}
            ).wait_recv()
        for k in range(1, NDP):
            total = total + precv[l, lax.rem(di + k, NDP)].astype(F32)
        some = trecv.at[l, pl.ds(0, NDP - 1)]
        remote(some, some, t_ss.at[l], t_rs.at[l], y_peer(1)[1]).wait_recv()
        squares = tsend[l, lax.div(di, 4)].astype(F32)
        for k in range(1, NDP):
            squares = squares + trecv[l, lax.rem(di + k, NDP)].astype(F32)
        squares = squares[0:1] + squares[1:2]
        picked = lax.broadcasted_iota(jnp.int32, (SEQ, 128), 1) == (
            lax.broadcasted_iota(jnp.int32, (SEQ, 128), 0) + SEQ * lax.rem(di, 4)
        )
        squares = jnp.sum(jnp.where(picked, squares, 0.0), axis=1, keepdims=True)
        total = total * lax.rsqrt(squares * (1.0 / D) + 1e-6)
        r, k_, v, pd, pa, pg = [total[:, 64 * p : 64 * p + 64] for p in range(6)]
        decay = jnp.exp(-0.6065306597126334 * jax.nn.sigmoid(floor_ref[l : l + 1, :] + pd))
        rate = jax.nn.sigmoid(pa)
        gate = jax.nn.sigmoid(pg)
        u = k_ * lax.rsqrt(jnp.sum(k_ * k_, axis=1, keepdims=True) + 1e-6)
        kr = k_ * rate
        ur = u * rate
        dr = decay * r
        row16 = lax.broadcasted_iota(jnp.int32, (16, 64), 0) % 8
        cs, ys = [], []
        for q in range(4):
            rows = slice(8 * q, 8 * q + 8)
            left = jnp.concatenate([u[rows], dr[rows]], axis=0).astype(BF16)
            res = lax.dot_general(left, stb[512 * q : 512 * q + 512], NT, preferred_element_type=F32)
            acc = jnp.zeros((16, 64), F32)
            for t in range(8):
                acc = jnp.where(row16 == t, res[:, 64 * t : 64 * t + 64], acc)
            cs.append(acc[0:8])
            ys.append(acc[8:16])
        c = -jnp.concatenate(cs, axis=0)
        y = (
            jnp.concatenate(ys, axis=0)
            + c * jnp.sum(ur * r, axis=1, keepdims=True)
            + v * jnp.sum(kr * r, axis=1, keepdims=True)
        )
        y = y - jnp.mean(y, axis=1, keepdims=True)
        var = jnp.mean(y * y, axis=1, keepdims=True)
        o = y * lax.rsqrt(var + 0.00064) * norm_ref[l : l + 1, :]
        o = o + jnp.sum(r * kr * direct_ref[l : l + 1, :], axis=1, keepdims=True) * v
        o = o * gate
        osend[l] = jnp.concatenate([o[0:16], o[16:32]], axis=1).astype(BF16)
        slot = yi * NC + ci
        for k in (4, 3, 5, 2, 6, 1, 7):
            remote(osend.at[l], oget.at[l, slot], o_ss.at[l], o_rs.at[l], {**dp_peer(k)[1], "y": xi}).start()

        @pl.when(yi != xi)
        def _():
            remote(osend.at[l], oget.at[l, slot], o_ss.at[l], o_rs.at[l], {"y": xi}).start()

        @pl.when(yi == xi)
        def _():
            oget[l, slot] = osend[l]

        if l == 0:
            wo_loads[1].wait()
            for k in (2, 1, 3):
                remote(wo.at[1, yi], wo.at[1, yi], w_ss.at[1], w_rs.at[1], y_peer(k)[1]).start()
        ct = c.T
        vt = v.T

        def update(lo, hi):
            for s in range(lo, hi):
                st_out[l, s] = (
                    st[l, s] * decay[s : s + 1, :]
                    + ct[:, s : s + 1] * ur[s : s + 1, :]
                    + vt[:, s : s + 1] * kr[s : s + 1, :]
                )

        with jax.named_scope("w_w"):
            some = wo.at[l, pl.ds(0, 3)]
            remote(some, some, w_ss.at[l], w_rs.at[l], y_peer(1)[1]).wait_recv()
        with jax.named_scope("w_o"):
            o_count(l, lambda some: remote(some, some, o_ss.at[l], o_rs.at[l], y_peer(1)[1]).wait_recv())

        left = []
        for p in range(NY):
            packed = [oget[l, p * NC + i] for i in range(NC)]
            left.append(jnp.concatenate([b[:, c0 : c0 + 64] for b in packed for c0 in (0, 64)], axis=0))
        share = lax.dot_general(
            jnp.concatenate(left, axis=1), wo[l].reshape(NY * HC, 512), NN, preferred_element_type=F32
        ).astype(BF16)
        for rg in range(8):
            for cg in range(4):
                zsend[l, order[rg % 4 * 4 + cg], rg // 4] = share[8 * rg : 8 * rg + 8, 128 * cg : 128 * cg + 128]
        if l == 0:
            with jax.named_scope("w_16"):
                pl.semaphore_wait(within16, 2)

        def z_scatter(k, _):
            src = zsend.at[l, jnp.where(k < 16, k, 31 - k)]
            remote(src, zrecv.at[l, zi], z_ss.at[l], z_rs.at[l], z_peer(far_first(k))[1]).start()
            return 0

        with jax.named_scope("zsend"):
            lax.fori_loop(0, NZ - 1, z_scatter, 0)
        zrecv[l, zi] = zsend[l, 0]
        with jax.named_scope("upd"):
            update(0, SEQ)
        with jax.named_scope("w_z"):
            some = zrecv.at[l, pl.ds(0, NZ - 1)]
            remote(some, some, z_ss.at[l], z_rs.at[l], z_peer(1)[1]).wait_recv()
        def pair(at):
            return hid.at[l + 1, yi, :, lax.rem(at, 16)]

        mine = jnp.sum(zrecv[l].astype(F32), axis=0)
        for h in range(2):
            hid[l + 1, yi, h, lax.rem(zi, 16)] = (mine[h] + hid[l, yi, h, lax.rem(zi, 16)].astype(F32)).astype(BF16)

        for g, (lo, hi) in enumerate(GROUPS):

            def z_gather(k, _):
                _, dev = z_peer(near_off(k))
                remote(pair(zi), pair(zi), g_ss.at[l], g_rs.at[l, g], dev).start()
                if g < DIRECT:
                    for i in (2, 1, 3):
                        both = {**dev, **y_peer(i)[1]}
                        remote(pair(zi), pair(zi), h_ss.at[l], h_rs.at[l], both).start()
                return 0

            with jax.named_scope("zsend"):
                lax.fori_loop(lo, hi, z_gather, 0)

        def forward(at):
            for k in (2, 1, 3):
                remote(pair(at), pair(at), h_ss.at[l], h_rs.at[l], y_peer(k)[1]).start()

        forward(zi)
        for g in range(len(GROUPS) - 1, -1, -1):
            lo, hi = GROUPS[g]
            with jax.named_scope("w_g"):
                some = zsend.at[l, pl.ds(0, hi - lo)]
                remote(some, some, g_ss.at[l], g_rs.at[l, g], z_peer(1)[1]).wait_recv()

            def onward(k, _):
                forward(zi + NZ - near_off(k))
                return 0

            if g >= DIRECT:
                with jax.named_scope("fwd"):
                    lax.fori_loop(lo, hi, onward, 0)
        three = hid.at[l + 1, pl.ds(0, 3)]
        with jax.named_scope("w_h"):
            remote(three, three, h_ss.at[l], h_rs.at[l], {"y": lax.rem(yi + 1, NY)}).wait_recv()

    hid_out[...] = hid[2]
    for l in range(2):
        near = {"y": lax.rem(yi + 1, NY)}
        for buf, ss in (
            (trecv.at[l, pl.ds(0, NDP - 1)], t_ss),
            (psend.at[l, pl.ds(0, NDP - 1)], p_ss),
            (wo.at[l, pl.ds(0, 3)], w_ss),
            (zrecv.at[l, pl.ds(0, NZ - 1)], z_ss),
            (zsend.at[l, pl.ds(0, 15)], g_ss),
            (hid.at[l, pl.ds(0, 3)], h_ss),
        ):
            remote(buf, buf, ss.at[l], p_rs.at[l], near).wait_send()
        o_count(l, lambda some: remote(some, some, o_ss.at[l], o_rs.at[l], near).wait_send())


def per_device(
    incoming_token, input_norm_gain, receptance_weight, key_weight, value_weight, decay_weight,
    learning_rate_weight, gate_weight, channel_decay_floor, direct_token_weight, head_norm_gain,
    output_weight, incoming_state,
):
    tiles = incoming_token.reshape(NZ, 8, 4, 128).transpose(0, 2, 1, 3).reshape(NY, 2, 16, 8, 128)
    weights = [
        jnp.swapaxes(w, 1, 2)
        for w in (
            receptance_weight, key_weight, value_weight, decay_weight, learning_rate_weight, gate_weight,
        )
    ]
    state = incoming_state.reshape(2, SEQ, HC, HC)
    anywhere = pl.BlockSpec(memory_space=pl.ANY)
    vmem = pl.BlockSpec(memory_space=pltpu.VMEM)
    dma = pltpu.SemaphoreType.DMA
    hidden, new_state = pl.pallas_call(
        kernel,
        out_shape=(
            pltpu.VMEM((NY, 2, 16, 8, 128), BF16),
            pltpu.VMEM((2, SEQ, HC, HC), F32),
        ),
        in_specs=[anywhere] * 13,
        out_specs=(vmem, vmem),
        scratch_shapes=[
            pltpu.VMEM((3, NY, 2, 16, 8, 128), BF16),
            pltpu.VMEM((2, 512), F32),
            *[pltpu.VMEM((2, HC), F32) for _ in range(3)],
            pltpu.VMEM((2, 384, 512), BF16),
            pltpu.VMEM((2, NY, HC, 512), BF16),
            pltpu.VMEM((2, SEQ, HC, HC), F32),
            pltpu.VMEM((SEQ * HC, HC), BF16),
            pltpu.VMEM((2, 2, 8, 128), BF16),
            pltpu.VMEM((2, NDP, 8, 128), BF16),
            pltpu.VMEM((2, NDP, SEQ, 384), BF16),
            pltpu.VMEM((2, NDP, SEQ, 384), BF16),
            pltpu.VMEM((2, 16, 128), BF16),
            pltpu.VMEM((2, NY * NC, 16, 128), BF16),
            pltpu.VMEM((2, 16, 2, 8, 128), BF16),
            pltpu.VMEM((2, NZ, 2, 8, 128), BF16),
            dma((21,)),
            *[dma((2,)) for _ in range(11)],
            dma((2, len(GROUPS))),
            *[dma((2,)) for _ in range(2)],
            pltpu.SemaphoreType.REGULAR,
            pltpu.SemaphoreType.REGULAR,
        ],
        compiler_params=pltpu.CompilerParams(
            collective_id=0, has_side_effects=True, vmem_limit_bytes=60 * 1024 * 1024
        ),
        name="decode_step",
    )(
        tiles, input_norm_gain, *weights, channel_decay_floor, direct_token_weight, head_norm_gain,
        output_weight, state,
    )
    hidden = hidden.reshape(NZ, 4, 8, 128).transpose(0, 2, 1, 3).reshape(256, 512)
    return (hidden, new_state.reshape(2, SEQ, 1, HC, HC))


def solution(mesh):
    finer = Mesh(mesh.devices.reshape(NZ, NY, NX, NC), ("z", "y", "x", "c"))
    tp, dp = ("z", "y"), ("x", "c")
    w = P(None, dp, tp)
    return jax.shard_map(
        per_device,
        mesh=finer,
        in_specs=(
            P(None, dp), P(None, dp), w, w, w, w, w, w, P(None, tp), P(None, tp), P(None, tp),
            P(None, tp, dp), P(None, dp, tp, None, None),
        ),
        out_specs=(P(None, dp), P(None, dp, tp, None, None)),
        check_vma=False,
    )
```

time: 107 us -> 99.1 us (0.926)
  the two profiles are of different devices: /device:TPU:8 before, /device:TPU:2 now
where the time goes in v3:
time: 99.1 us; the launch traced here: 98.9 us
  Pallas kernels  96.3 us (97%)
  local copies, waits for them, and re-layouts  2.02 us (2%)
    pallas_call x1, Pallas kernels, per_device(): pl.pallas_call(kernel, out_shape=(pltpu.VMEM((NY, 2, 16, 8, 128), BF16),...  96.3 us
    unnamed x2, local copies, waits for them, and re-layouts  2.02 us

profile of v3, /device:TPU:2, one launch (start us, length us, event | category | flops | bytes accessed | tf_op | source)
XLA Modules:
  0.0 98.9 jit_solution(5156472886571093756)
XLA Ops:
  0.6 96.3 %decode_step.1 = (bf16[4,2,16,8,128]{4,3,2,1,0:T(8,128)(2,1)S(1)}, f32[2,32,64,64]{3,2,1,0:T(8,128)S(1)}) custom-call(bf16[4,2,16,8,128]{4,3,2,1,0:T(8,128)(2,1)} %bitcast.23, f32[2,512]{1,0:T(2,128)} %gain_hbm.1, bf16[2,64,512]{2,1,0:T(8,128)(2,1)} %bitcast.24, bf16[2,64,512]{2,1,0:T(8,128)(2,1)} %bitcast.25, bf16[2,64,512]{2,1,0:T(8,128)(2,1)} %bitcast.26, ...), custom_call_target="tpu_custom_call" | custom-call | tf_op jit(solution)/shard_map/decode_step/pallas_call | solution.py:340
  96.9 0.7 copy.18
  97.6 1.3 %copy.19 = f32[2,32,1,64,64]{4,3,2,1,0:T(8,128)} copy(f32[2,32,1,64,64]{4,3,2,1,0:T(8,128)S(1)} %bitcast.20) | data formatting | bytes 2097152

commit v4 on v3

--- a/solution.py
+++ b/solution.py
@@ -26,11 +26,15 @@
     tok_hbm, gain_hbm, wr, wk, wv, wd, wa, wg, floor_hbm, direct_hbm, norm_hbm, wo_hbm, st_hbm,
     hid_out, st_out,
     hid, gain_ref, floor_ref, direct_ref, norm_ref, wt, wo, st, stb, tsend, trecv, psend, precv, osend, oget, zsend, zrecv,
-    load_sem, t_ss, t_rs, p_ss, p_rs, o_ss, o_rs, w_ss, w_rs, z_ss, z_rs, g_ss, g_rs, h_ss, h_rs, within8, within16,
+    load_sem, t_ss, t_rs, p_ss, p_rs, o_ss, o_rs, w_ss, w_rs, z_ss, z_rs, g_ss, g_rs, h_ss, h_rs, m_sem, within8, within16,
 ):
     zi, yi = lax.axis_index("z"), lax.axis_index("y")
     xi, ci = lax.axis_index("x"), lax.axis_index("c")
     di = xi * NC + ci
+    odd = lax.rem(zi, 2)
+    mate = {"z": zi + 1 - 2 * odd}
+    place = lax.div(zi, 2)
+    own_head, mate_head = odd * NY + yi, (1 - odd) * NY + yi
 
     def dp_peer(k):
         d = lax.rem(di + k, NDP)
@@ -50,24 +54,26 @@
         )
 
     def far_first(k):
-        return jnp.where(k % 2 == 0, NZ // 2 + k // 2, NZ // 2 - (k + 1) // 2)
+        return jnp.where(k % 2 == 0, 8 + k // 2, 8 - (k + 1) // 2)
 
     def near_off(k):
         return jnp.where(k % 2 == 0, NZ - 8 + k // 2, 8 - (k + 1) // 2)
 
+    def wo_gather():
+        own = wo.at[0, own_head]
+        for dev in (y_peer(2)[1], {**y_peer(2)[1], **mate}, mate, *[{**y_peer(k)[1], **m} for k in (1, 3) for m in ({}, mate)]):
+            remote(own, own, w_ss.at[0], w_rs.at[0], dev).start()
+
+    o_home = (yi == xi) & (odd == ci)
+
     def o_count(l, wait):
-        @pl.when(yi != xi)
+        @pl.when(jnp.logical_not(o_home))
         def _():
             wait(oget.at[l])
 
-        @pl.when(yi == xi)
+        @pl.when(o_home)
         def _():
             wait(oget.at[l, pl.ds(0, NDP - 1)])
-
-    order = []
-    for q in range(16):
-        apart = lax.rem(q + NZ - zi, 16)
-        order.append(jnp.where(apart < 8, 2 * apart, 31 - 2 * apart))
 
     barrier = pltpu.get_barrier_semaphore()
 
@@ -77,6 +83,9 @@
         pl.semaphore_signal(barrier, inc=1, device_id=dp_peer(k)[1], device_id_type=MESH)
     for k in range(1, NY):
         pl.semaphore_signal(barrier, inc=1, device_id=y_peer(k)[1], device_id_type=MESH)
+        pl.semaphore_signal(barrier, inc=1, device_id={**y_peer(k)[1], **mate}, device_id_type=MESH)
+
+    to_mate = remote(wo.at[1, own_head], wo.at[1, own_head], m_sem.at[0], m_sem.at[1], mate)
 
     loads = [pltpu.make_async_copy(tok_hbm, hid.at[0], load_sem.at[0])]
     for l in range(2):
@@ -85,7 +94,7 @@
                 pltpu.make_async_copy(w.at[l], wt.at[l, pl.ds(64 * p, 64)], load_sem.at[1 + 6 * l + p])
             )
     state_loads = [pltpu.make_async_copy(st_hbm.at[l], st.at[l], load_sem.at[13 + l]) for l in range(2)]
-    wo_loads = [pltpu.make_async_copy(wo_hbm.at[l], wo.at[l, yi], load_sem.at[15 + 5 * l]) for l in range(2)]
+    wo_loads = [pltpu.make_async_copy(wo_hbm.at[l], wo.at[l, own_head], load_sem.at[15 + 5 * l]) for l in range(2)]
     smalls = [
         pltpu.make_async_copy(a, b, load_sem.at[16 + i])
         for i, (a, b) in enumerate(
@@ -133,7 +142,9 @@
         psend[l] = proj.reshape(NDP, SEQ, 384)
         if l == 0:
             with jax.named_scope("w_bar"):
-                pl.semaphore_wait(barrier, 8 + (NDP - 1) + (NY - 1))
+                pl.semaphore_wait(barrier, 8 + (NDP - 1) + 2 * (NY - 1))
+            wo_loads[0].wait()
+            wo_gather()
             for k in (4, NZ - 4):
                 pl.semaphore_signal(within8, inc=1, device_id=z_peer(k)[1], device_id_type=MESH)
         for k in (4, 3, 5, 2, 6, 1, 7):
@@ -143,9 +154,8 @@
             d, dev = dp_peer(k)
             remote(psend.at[l, d], precv.at[l, di], p_ss.at[l], p_rs.at[l], dev).start()
         if l == 0:
-            wo_loads[0].wait()
-            for k in (2, 1, 3):
-                remote(wo.at[0, yi], wo.at[0, yi], w_ss.at[0], w_rs.at[0], y_peer(k)[1]).start()
+            wo_loads[1].wait()
+            to_mate.start()
         with jax.named_scope("w_st"):
             state_loads[l].wait()
         stb[...] = st[l].reshape(SEQ * HC, HC).astype(BF16)
@@ -203,22 +213,18 @@
         o = o + jnp.sum(r * kr * direct_ref[l : l + 1, :], axis=1, keepdims=True) * v
         o = o * gate
         osend[l] = jnp.concatenate([o[0:16], o[16:32]], axis=1).astype(BF16)
-        slot = yi * NC + ci
+        there = {"y": xi, "z": zi - odd + ci}
         for k in (4, 3, 5, 2, 6, 1, 7):
-            remote(osend.at[l], oget.at[l, slot], o_ss.at[l], o_rs.at[l], {**dp_peer(k)[1], "y": xi}).start()
-
-        @pl.when(yi != xi)
+            remote(osend.at[l], oget.at[l, own_head], o_ss.at[l], o_rs.at[l], {**dp_peer(k)[1], **there}).start()
+
+        @pl.when(jnp.logical_not(o_home))
         def _():
-            remote(osend.at[l], oget.at[l, slot], o_ss.at[l], o_rs.at[l], {"y": xi}).start()
-
-        @pl.when(yi == xi)
+            remote(osend.at[l], oget.at[l, own_head], o_ss.at[l], o_rs.at[l], there).start()
+
+        @pl.when(o_home)
         def _():
-            oget[l, slot] = osend[l]
-
-        if l == 0:
-            wo_loads[1].wait()
-            for k in (2, 1, 3):
-                remote(wo.at[1, yi], wo.at[1, yi], w_ss.at[1], w_rs.at[1], y_peer(k)[1]).start()
+            oget[l, own_head] = osend[l]
+
         ct = c.T
         vt = v.T
 
@@ -231,44 +237,51 @@
                 )
 
         with jax.named_scope("w_w"):
-            some = wo.at[l, pl.ds(0, 3)]
+            some = wo.at[l, pl.ds(0, 7 - l)]
             remote(some, some, w_ss.at[l], w_rs.at[l], y_peer(1)[1]).wait_recv()
         with jax.named_scope("w_o"):
             o_count(l, lambda some: remote(some, some, o_ss.at[l], o_rs.at[l], y_peer(1)[1]).wait_recv())
 
         left = []
-        for p in range(NY):
-            packed = [oget[l, p * NC + i] for i in range(NC)]
-            left.append(jnp.concatenate([b[:, c0 : c0 + 64] for b in packed for c0 in (0, 64)], axis=0))
+        for p in range(2 * NY):
+            packed = oget[l, p]
+            left.append(jnp.concatenate([packed[:, 0:64], packed[:, 64:128]], axis=0))
         share = lax.dot_general(
-            jnp.concatenate(left, axis=1), wo[l].reshape(NY * HC, 512), NN, preferred_element_type=F32
+            jnp.concatenate(left, axis=1), wo[l].reshape(2 * NY * HC, 512), NN, preferred_element_type=F32
         ).astype(BF16)
-        for rg in range(8):
-            for cg in range(4):
-                zsend[l, order[rg % 4 * 4 + cg], rg // 4] = share[8 * rg : 8 * rg + 8, 128 * cg : 128 * cg + 128]
+        for n in range(16):
+            rg, cg = n // 4, n % 4
+            zsend[l, n % 8, n // 8] = share[8 * rg : 8 * rg + 8, 128 * cg : 128 * cg + 128]
         if l == 0:
             with jax.named_scope("w_16"):
                 pl.semaphore_wait(within16, 2)
 
         def z_scatter(k, _):
-            src = zsend.at[l, jnp.where(k < 16, k, 31 - k)]
-            remote(src, zrecv.at[l, zi], z_ss.at[l], z_rs.at[l], z_peer(far_first(k))[1]).start()
+            p, dev = z_peer(2 * far_first(k))
+            src = zsend.at[l, lax.rem(lax.div(p, 2), 8)]
+            remote(src, zrecv.at[l, place], z_ss.at[l], z_rs.at[l], dev).start()
             return 0
 
         with jax.named_scope("zsend"):
-            lax.fori_loop(0, NZ - 1, z_scatter, 0)
-        zrecv[l, zi] = zsend[l, 0]
+            lax.fori_loop(0, 15, z_scatter, 0)
+        if l == 0:
+            to_mate.wait_recv()
+            for k in (2, 1, 3):
+                for head in (own_head, mate_head):
+                    remote(wo.at[1, head], wo.at[1, head], w_ss.at[1], w_rs.at[1], y_peer(k)[1]).start()
+        zrecv[l, place] = zsend[l, lax.rem(place, 8)]
         with jax.named_scope("upd"):
             update(0, SEQ)
         with jax.named_scope("w_z"):
-            some = zrecv.at[l, pl.ds(0, NZ - 1)]
+            some = zrecv.at[l, pl.ds(0, 15)]
             remote(some, some, z_ss.at[l], z_rs.at[l], z_peer(1)[1]).wait_recv()
         def pair(at):
-            return hid.at[l + 1, yi, :, lax.rem(at, 16)]
+            return hid.at[l + 1, yi, lax.rem(at, 2), :, lax.rem(lax.div(at, 2), 8)]
 
         mine = jnp.sum(zrecv[l].astype(F32), axis=0)
         for h in range(2):
-            hid[l + 1, yi, h, lax.rem(zi, 16)] = (mine[h] + hid[l, yi, h, lax.rem(zi, 16)].astype(F32)).astype(BF16)
+            q = lax.rem(place, 8)
+            hid[l + 1, yi, odd, h, q] = (mine[h] + hid[l, yi, odd, h, q].astype(F32)).astype(BF16)
 
         for g, (lo, hi) in enumerate(GROUPS):
 
@@ -292,7 +305,7 @@
         for g in range(len(GROUPS) - 1, -1, -1):
             lo, hi = GROUPS[g]
             with jax.named_scope("w_g"):
-                some = zsend.at[l, pl.ds(0, hi - lo)]
+                some = zrecv.at[l, pl.ds(0, hi - lo)]
                 remote(some, some, g_ss.at[l], g_rs.at[l, g], z_peer(1)[1]).wait_recv()
 
             def onward(k, _):
@@ -307,14 +320,15 @@
             remote(three, three, h_ss.at[l], h_rs.at[l], {"y": lax.rem(yi + 1, NY)}).wait_recv()
 
     hid_out[...] = hid[2]
+    to_mate.wait_send()
     for l in range(2):
         near = {"y": lax.rem(yi + 1, NY)}
         for buf, ss in (
             (trecv.at[l, pl.ds(0, NDP - 1)], t_ss),
             (psend.at[l, pl.ds(0, NDP - 1)], p_ss),
-            (wo.at[l, pl.ds(0, 3)], w_ss),
-            (zrecv.at[l, pl.ds(0, NZ - 1)], z_ss),
-            (zsend.at[l, pl.ds(0, 15)], g_ss),
+            (wo.at[l, pl.ds(0, 7 - l)], w_ss),
+            (zrecv.at[l, pl.ds(0, 15)], z_ss),
+            (zrecv.at[l, pl.ds(0, 15)], g_ss),
             (hid.at[l, pl.ds(0, 3)], h_ss),
         ):
             remote(buf, buf, ss.at[l], p_rs.at[l], near).wait_send()
@@ -326,7 +340,7 @@
     learning_rate_weight, gate_weight, channel_decay_floor, direct_token_weight, head_norm_gain,
     output_weight, incoming_state,
 ):
-    tiles = incoming_token.reshape(NZ, 8, 4, 128).transpose(0, 2, 1, 3).reshape(NY, 2, 16, 8, 128)
+    tiles = incoming_token.reshape(NZ, 8, 4, 128).transpose(0, 2, 1, 3).reshape(NY, 2, 2, 8, 8, 128)
     weights = [
         jnp.swapaxes(w, 1, 2)
         for w in (
@@ -340,17 +354,17 @@
     hidden, new_state = pl.pallas_call(
         kernel,
         out_shape=(
-            pltpu.VMEM((NY, 2, 16, 8, 128), BF16),
+            pltpu.VMEM((NY, 2, 2, 8, 8, 128), BF16),
             pltpu.VMEM((2, SEQ, HC, HC), F32),
         ),
         in_specs=[anywhere] * 13,
         out_specs=(vmem, vmem),
         scratch_shapes=[
-            pltpu.VMEM((3, NY, 2, 16, 8, 128), BF16),
+            pltpu.VMEM((3, NY, 2, 2, 8, 8, 128), BF16),
             pltpu.VMEM((2, 512), F32),
             *[pltpu.VMEM((2, HC), F32) for _ in range(3)],
             pltpu.VMEM((2, 384, 512), BF16),
-            pltpu.VMEM((2, NY, HC, 512), BF16),
+            pltpu.VMEM((2, 2 * NY, HC, 512), BF16),
             pltpu.VMEM((2, SEQ, HC, HC), F32),
             pltpu.VMEM((SEQ * HC, HC), BF16),
             pltpu.VMEM((2, 2, 8, 128), BF16),
@@ -359,12 +373,13 @@
             pltpu.VMEM((2, NDP, SEQ, 384), BF16),
             pltpu.VMEM((2, 16, 128), BF16),
             pltpu.VMEM((2, NY * NC, 16, 128), BF16),
+            pltpu.VMEM((2, 8, 2, 8, 128), BF16),
             pltpu.VMEM((2, 16, 2, 8, 128), BF16),
-            pltpu.VMEM((2, NZ, 2, 8, 128), BF16),
             dma((21,)),
             *[dma((2,)) for _ in range(11)],
             dma((2, len(GROUPS))),
             *[dma((2,)) for _ in range(2)],
+            dma((2,)),
             pltpu.SemaphoreType.REGULAR,
             pltpu.SemaphoreType.REGULAR,
         ],

time: 99.1 us -> 93.8 us (0.947)
  the two profiles are of different devices: /device:TPU:2 before, /device:TPU:8 now
where the time goes in v4:
time: 93.8 us; the launch traced here: 93.6 us
  Pallas kernels  91 us (97%)
  local copies, waits for them, and re-layouts  2.02 us (2%)
    pallas_call x1, Pallas kernels, per_device(): pl.pallas_call(kernel, out_shape=(pltpu.VMEM((NY, 2, 2, 8, 8, 128), BF16)...  91 us
    unnamed x2, local copies, waits for them, and re-layouts  2.02 us

profile of v4, /device:TPU:8, one launch (start us, length us, event | category | flops | bytes accessed | tf_op | source)
XLA Modules:
  0.0 93.6 jit_solution(14998958235089447775)
XLA Ops:
  0.6 91.0 %decode_step.1 = (bf16[4,2,2,8,8,128]{5,4,3,2,1,0:T(8,128)(2,1)S(1)}, f32[2,32,64,64]{3,2,1,0:T(8,128)S(1)}) custom-call(bf16[4,2,2,8,8,128]{5,4,3,2,1,0:T(8,128)(2,1)} %bitcast.23, f32[2,512]{1,0:T(2,128)} %gain_hbm.1, bf16[2,64,512]{2,1,0:T(8,128)(2,1)} %bitcast.24, bf16[2,64,512]{2,1,0:T(8,128)(2,1)} %bitcast.25, bf16[2,64,512]{2,1,0:T(8,128)(2,1)} %bitcast.26, ...), custom_call_target="tpu_custom_call" | custom-call | tf_op jit(solution)/shard_map/decode_step/pallas_call | solution.py:354
  91.6 0.7 copy.18
  92.3 1.3 %copy.19 = f32[2,32,1,64,64]{4,3,2,1,0:T(8,128)} copy(f32[2,32,1,64,64]{4,3,2,1,0:T(8,128)S(1)} %bitcast.20) | data formatting | bytes 2097152

commit v5 on v4

--- a/solution.py
+++ b/solution.py
@@ -333,6 +333,17 @@
         ):
             remote(buf, buf, ss.at[l], p_rs.at[l], near).wait_send()
         o_count(l, lambda some: remote(some, some, o_ss.at[l], o_rs.at[l], near).wait_send())
+
+
+def finish(hid_ref, st_ref, hid_out, st_out, sem):
+    copies = [pltpu.make_async_copy(hid_ref, hid_out, sem.at[8])]
+    for i in range(8):
+        part = (i // 4, pl.ds(8 * (i % 4), 8))
+        copies.append(pltpu.make_async_copy(st_ref.at[part], st_out.at[part], sem.at[i]))
+    for cp in copies:
+        cp.start()
+    for cp in copies:
+        cp.wait()
 
 
 def per_device(
@@ -391,6 +402,18 @@
         tiles, input_norm_gain, *weights, channel_decay_floor, direct_token_weight, head_norm_gain,
         output_weight, state,
     )
+    hidden, new_state = pl.pallas_call(
+        finish,
+        out_shape=(
+            jax.ShapeDtypeStruct(hidden.shape, BF16),
+            jax.ShapeDtypeStruct(new_state.shape, F32),
+        ),
+        in_specs=[vmem, vmem],
+        out_specs=(anywhere, anywhere),
+        scratch_shapes=[dma((9,))],
+        compiler_params=pltpu.CompilerParams(vmem_limit_bytes=8 * 1024 * 1024),
+        name="finish",
+    )(hidden, new_state)
     hidden = hidden.reshape(NZ, 4, 8, 128).transpose(0, 2, 1, 3).reshape(256, 512)
     return (hidden, new_state.reshape(2, SEQ, 1, HC, HC))
 

time: 93.8 us -> 93.2 us (level)
  local copies, waits for them, and re-layouts: 2.02 us -> 0 us
  Pallas kernels: 91 us -> 92.4 us
    unnamed x2 -> x0, local copies, waits for them, and re-layouts: 2.02 us -> none
    pallas_call x0 -> x1, Pallas kernels: none -> 1.47 us  [per_device(): pl.pallas_call(finish, out_shape=(jax.ShapeDtypeStruct(hidden.shape, BF16...]
where the time goes in v5:
time: 93.2 us; the launch traced here: 93.1 us
  Pallas kernels  92.4 us (99%)
    pallas_call x1, Pallas kernels, per_device(): pl.pallas_call(kernel, out_shape=(pltpu.VMEM((NY, 2, 2, 8, 8, 128), BF16)...  91 us

profile of v5, /device:TPU:8, one launch (start us, length us, event | category | flops | bytes accessed | tf_op | source)
XLA Modules:
  0.0 93.1 jit_solution(1431975790530405873)
XLA Ops:
  0.6 91.0 %decode_step.1 = (bf16[4,2,2,8,8,128]{5,4,3,2,1,0:T(8,128)(2,1)S(1)}, f32[2,32,64,64]{3,2,1,0:T(8,128)S(1)}) custom-call(bf16[4,2,2,8,8,128]{5,4,3,2,1,0:T(8,128)(2,1)} %bitcast.21, f32[2,512]{1,0:T(2,128)} %gain_hbm.1, bf16[2,64,512]{2,1,0:T(8,128)(2,1)} %bitcast.22, bf16[2,64,512]{2,1,0:T(8,128)(2,1)} %bitcast.23, bf16[2,64,512]{2,1,0:T(8,128)(2,1)} %bitcast.24, ...), custom_call_target="tpu_custom_call" | custom-call | tf_op jit(solution)/shard_map/decode_step/pallas_call | solution.py:365
  91.6 1.5 %finish.1 = (bf16[4,2,2,8,8,128]{5,4,3,2,1,0:T(8,128)(2,1)}, f32[2,32,64,64]{3,2,1,0:T(8,128)}) custom-call(bf16[4,2,2,8,8,128]{5,4,3,2,1,0:T(8,128)(2,1)S(1)} %get-tuple-element.6.hid_ref, f32[2,32,64,64]{3,2,1,0:T(8,128)S(1)} %get-tuple-element.7.st_ref), custom_call_target="tpu_custom_call" | custom-call | tf_op jit(solution)/shard_map/finish/pallas_call | solution.py:405
